TPU v7x, 32 devices: a whole 2x2x4 slice. The times are simulated.
32 devices in a mesh: sp: 8 (over z, y), tp: 4 (over x, core).
Axes of the slice: x: 2, y: 2, z: 4, core: 2. Of those that a mesh axis runs over, the one named last changes fastest.
Arguments:
- hidden_state: bfloat16 [1024, 2048], P('sp'), may hold values from -6 to 6
- out_grad: bfloat16 [1024, 2048], P('sp'), may hold values from -8 to 8
- routes: int32 [1024, 2], P('sp'), may hold values from 0 to 3, all different within a row; in each aligned block of 128 rows (0 to 127, 128 to 255, ...) at most 96 rows name the same one
- route_weights: float32 [1024, 2], P('sp'), may hold values from 0.25 to 1
- w_gate: bfloat16 [8, 2048, 1792], P('sp', None, 'tp'), may hold values from -0.125 to 0.125
- w_up: bfloat16 [8, 2048, 1792], P('sp', None, 'tp'), may hold values from -0.125 to 0.125
- w_down: bfloat16 [8, 1792, 2048], P('sp', 'tp'), may hold values from -0.09375 to 0.09375
- value: bfloat16 [1024, 512], P('sp', 'tp'), may hold values from -6 to 6
- gate_in: bfloat16 [1024, 512], P('sp', 'tp'), may hold values from -6 to 6
- normed: bfloat16 [1024, 512], P('sp', 'tp'), may hold values from -24 to 24
- inv_std: float32 [1024], P('sp'), may hold values from 0.5 to 2
- norm_gain: float32 [512], P('tp'), may hold values from 0.1 to 1.9
- taps: float32 [31, 512], P(None, 'tp'), may hold values from -1 to 1
- w_proj: bfloat16 [2048, 512], P(None, 'tp'), may hold values from -0.25 to 0.25
Outputs:
- w_gate_grad: bfloat16 [8, 2048, 1792], P('sp', None, 'tp')
- w_up_grad: bfloat16 [8, 2048, 1792], P('sp', None, 'tp')
- w_down_grad: bfloat16 [8, 1792, 2048], P('sp', 'tp')
- stream_grad: bfloat16 [1024, 2048], P('sp', 'tp')
- proj_grad: float32 [2048, 512], P('sp', 'tp')
- value_grad: bfloat16 [1024, 512], P('sp', 'tp')
- gate_in_grad: bfloat16 [1024, 512], P('sp', 'tp')
Inputs may be any that keep to these rules, and one draw needn't show every extreme that they name: `routes`: among the choices of one device's tokens no expert is named more than 96 times, a bound that some block reaches on some device; a token's choices differ.
All inputs are finite; a program needn't handle non-finite values.
Results may differ from a plain program's by a relative error of at most 0.0057.
Values may be sent and summed in bfloat16 or wider, within the bound.
A program may use at most 128 MiB of HBM per device.

v0:
```python
import functools

import jax
import jax.numpy as jnp
from jax import lax
from jax.experimental import pallas as pl
from jax.experimental.pallas import tpu as pltpu
from jax.sharding import PartitionSpec as P

GROUP = 2
PAIR = 2
MESH = pl.DeviceIdType.MESH
F32 = jnp.float32
BF16 = jnp.bfloat16


def dot_rows(a, b):
    return lax.dot_general(a, b, (((0,), (0,)), ((), ())), preferred_element_type=F32)


def dot_cols(a, b):
    return lax.dot_general(a, b, (((1,), (1,)), ((), ())), preferred_element_type=F32)


def place():
    s, t = lax.axis_index("sp"), lax.axis_index("tp")
    e, g = s // GROUP, s % GROUP
    hi, lo = t // PAIR, t % PAIR
    across = (s, (1 - hi) * PAIR + lo)
    beside = (e * GROUP + 1 - g, t)
    partner = (s, hi * PAIR + 1 - lo)
    return s, t, e, g, hi, lo, across, beside, partner


def greet(devices):
    barrier = pltpu.get_barrier_semaphore()
    for device in devices:
        pl.semaphore_signal(barrier, inc=1, device_id=device, device_id_type=MESH)
    pl.semaphore_wait(barrier, len(devices))


def remote(src, dst, send, recv, device):
    return pltpu.make_async_remote_copy(
        src_ref=src, dst_ref=dst, send_sem=send, recv_sem=recv, device_id=device, device_id_type=MESH
    )


def one_hot(rank_row, cap):
    slots = lax.broadcasted_iota(jnp.int32, (cap, rank_row.shape[1]), 0)
    return jnp.where(slots == rank_row, 1.0, 0.0)


def mega_kernel(
    experts, cap, ksize,
    h_ref, cot_ref, rank_ref, w_ref, gate_hbm, up_hbm, down_hbm,
    value_ref, gate_ref, normed_ref, std_ref, gain_ref, taps_ref, proj_ref,
    gw_hbm, uw_hbm, dw_hbm, stream_ref, pgrad_ref, vgrad_ref, ggrad_ref,
    buf, pack, wg, wu, wd, act, gg, ug, grad_ref, gw, uw, dw,
    from_core, sums, rx_a, ry_b, relay, rx2, back, done, full, stats, ext, pg, py, pz_out, pz,
    w_sem, o_sem, d_send, d_recv, g_send, g_recv,
    core_send, core_recv, hop_send, hop_recv, z_send, z_recv, t_send, t_recv, p_send, p_recv, q_send, q_recv,
):
    s, t, e, g, hi, lo, across, beside, partner = place()
    sp_ways = experts * GROUP
    tok, quarter = cot_ref.shape
    half = quarter // 2
    tp_ways = stats.shape[0]
    across_t, other_t = across[1], partner[1]
    far_t = (1 - hi) * PAIR + 1 - lo
    far = (s, far_t)
    z_peers = [(lax.rem(e + j, experts) * GROUP + g, t) for j in range(1, experts)]
    before = (lax.rem(s + sp_ways - 1, sp_ways), t)
    after = (lax.rem(s + 1, sp_ways), t)
    loads = [
        pltpu.make_async_copy(src, dst, w_sem.at[n])
        for n, (src, dst) in enumerate(((gate_hbm, wg), (up_hbm, wu), (down_hbm, wd)))
    ]
    for copy in loads:
        copy.start()
    sent = []

    def go(copy):
        copy.start()
        sent.append(copy)

    def cols_of(col):
        return pl.ds(pl.multiple_of(col * quarter, quarter), quarter)

    def source_of(j):
        return lax.rem(e + experts - j, experts)

    def rows_of(j):
        return pl.ds(pl.multiple_of(source_of(j) * GROUP * cap, cap), GROUP * cap)

    def loc(j, side, col):
        return pl.ds(pl.multiple_of((source_of(j) * GROUP + side) * cap, cap), cap), cols_of(col)

    own_rows, own_cols = loc(0, g, t)

    def d_copy(j):
        return remote(pack.at[j], buf.at[:, own_rows, own_cols], d_send.at[j], d_recv.at[j], z_peers[j - 1])

    greeted = False
    for j in list(range(1, experts)) + [0]:
        target = lax.rem(e + j, experts)
        hot = one_hot(rank_ref[pl.ds(target, 1), :], cap)
        scale = jnp.sum(hot * w_ref[pl.ds(target, 1), :], axis=1, keepdims=True)
        hot = hot.astype(BF16)
        rows = jnp.dot(hot, h_ref[...], preferred_element_type=F32).astype(BF16)
        cots = (jnp.dot(hot, cot_ref[...], preferred_element_type=F32) * scale).astype(BF16)
        if j:
            pack[j, 0] = rows
            pack[j, 1] = cots
            if not greeted:
                greet(z_peers + [across, beside, partner, far, before, after])
                greeted = True
            go(d_copy(j))
        else:
            buf[0, own_rows, own_cols] = rows
            buf[1, own_rows, own_cols] = cots

    def hop(n, j, ref, device):
        return remote(ref, ref, g_send.at[j, n], g_recv.at[j, n], device)

    def both(j, side, col):
        rows, cols = loc(j, side, col)
        return buf.at[:, rows, cols]

    def one_of(k, j, side, col):
        rows, cols = loc(j, side, col)
        return buf.at[k, rows, cols]

    def arrived(n, j, ref):
        hop(n, j, ref, partner).wait_recv()

    def d_first(j):
        block = both(j, g, t)
        if j:
            remote(block, block, d_send.at[j], d_recv.at[j], partner).wait_recv()
        go(hop(0, j, block, across))
        go(hop(1, j, block, beside))
        go(hop(2, j, block, partner))

    def d_second(j):
        arrived(0, j, both(j, g, across_t))
        go(hop(3, j, one_of(0, j, g, across_t), beside))
        go(hop(5, j, both(j, g, across_t), partner))
        arrived(1, j, both(j, 1 - g, t))
        go(hop(4, j, one_of(1, j, 1 - g, t), across))
        go(hop(6, j, both(j, 1 - g, t), partner))

    def d_third(j):
        arrived(3, j, one_of(0, j, 1 - g, across_t))
        go(hop(7, j, one_of(0, j, 1 - g, across_t), partner))
        arrived(4, j, one_of(1, j, 1 - g, across_t))
        go(hop(8, j, one_of(1, j, 1 - g, across_t), partner))

    def d_last(j):
        arrived(2, j, both(j, g, other_t))
        arrived(5, j, both(j, g, far_t))
        arrived(6, j, both(j, 1 - g, other_t))
        arrived(7, j, one_of(0, j, 1 - g, far_t))
        arrived(8, j, one_of(1, j, 1 - g, far_t))

    def compute(j):
        rows = rows_of(j)
        in_rows = buf[0, rows, :]
        in_cots = buf[1, rows, :]
        pre_gate = jnp.dot(in_rows, wg[...], preferred_element_type=F32)
        pre_up = jnp.dot(in_rows, wu[...], preferred_element_type=F32)
        gate_sig = jax.nn.sigmoid(pre_gate)
        silu_gate = pre_gate * gate_sig
        act_grad = dot_cols(in_cots, wd[...])
        gate_grad = (act_grad * pre_up * gate_sig * (1.0 + pre_gate * (1.0 - gate_sig))).astype(BF16)
        up_grad = (act_grad * silu_gate).astype(BF16)
        act[rows, :] = (silu_gate * pre_up).astype(BF16)
        gg[rows, :] = gate_grad
        ug[rows, :] = up_grad
        grad_ref[rows, :] = (dot_cols(gate_grad, wg[...]) + dot_cols(up_grad, wu[...])).astype(BF16)

    width = full.shape[1]
    piece = 256
    per_item = width // piece // 4

    def weight_item(which, n):
        @pl.loop(n * per_item, (n + 1) * per_item)
        def _(i):
            cols = pl.ds(pl.multiple_of(i * piece, piece), piece)
            if which == 0:
                gw[cols, :] = dot_rows(buf[0, :, cols], gg[...]).astype(BF16)
            elif which == 1:
                uw[cols, :] = dot_rows(buf[0, :, cols], ug[...]).astype(BF16)
            else:
                dw[:, cols] = dot_rows(act[...], buf[1, :, cols]).astype(BF16)

    stores = [
        pltpu.make_async_copy(src, dst, o_sem.at[n])
        for n, (src, dst) in enumerate(((gw, gw_hbm), (uw, uw_hbm), (dw, dw_hbm)))
    ]
    items = [(which, n) for which in range(3) for n in range(4)]

    def fill(count=1):
        for _ in range(count):
            if items:
                which, n = items.pop(0)
                weight_item(which, n)
                if n == 3:
                    stores[which].start()

    def core_copy(j, h, lane):
        return remote(
            grad_ref.at[rows_of(j), cols_of(h * PAIR + lane)],
            from_core.at[j, h], core_send.at[j, h], core_recv.at[j, h], partner,
        )

    def hop_copy(n, j, src, dst, device):
        return remote(src, dst, hop_send.at[j, n], hop_recv.at[j, n], device)

    def x_first(j):
        return hop_copy(0, j, sums.at[0, j, 1 - hi], rx_a.at[j], across)

    def y_first(j):
        return hop_copy(1, j, sums.at[1, j, :, 1 - g], ry_b.at[j], beside)

    def y_second(j):
        return hop_copy(2, j, relay.at[0, j], rx2.at[0, j], beside)

    def x_second(j):
        return hop_copy(3, j, relay.at[1, j], rx2.at[1, j], across)

    def z_copy(j):
        return remote(done.at[j], back.at[j], z_send.at[j], z_recv.at[j], (source_of(j) * GROUP + g, t))

    def first(j):
        for h in range(PAIR):
            core_copy(j, h, lo).wait_recv()
            mine = grad_ref[rows_of(j), cols_of(h * PAIR + lo)].astype(F32)
            total = (mine + from_core[j, h].astype(F32)).astype(BF16).reshape(GROUP, cap, quarter)
            sums[0, j, h] = total[:, :, :half]
            sums[1, j, h] = total[:, :, half:]
        go(x_first(j))
        go(y_first(j))

    def second(j):
        x_first(j).wait_recv()
        relay[0, j] = (sums[0, j, hi, 1 - g].astype(F32) + rx_a[j, 1 - g].astype(F32)).astype(BF16)
        go(y_second(j))
        y_first(j).wait_recv()
        relay[1, j] = (sums[1, j, 1 - hi, g].astype(F32) + ry_b[j, 1 - hi].astype(F32)).astype(BF16)
        go(x_second(j))

    def third(j):
        y_second(j).wait_recv()
        done[j, :, :half] = (
            sums[0, j, hi, g].astype(F32) + rx_a[j, g].astype(F32) + rx2[0, j].astype(F32)
        ).astype(BF16)
        x_second(j).wait_recv()
        done[j, :, half:] = (
            sums[1, j, hi, g].astype(F32) + ry_b[j, hi].astype(F32) + rx2[1, j].astype(F32)
        ).astype(BF16)
        if j:
            go(z_copy(j))

    step = max(1, experts // 4)
    chunks = [list(range(c, min(c + step, experts))) for c in range(0, experts, step)]

    def returns(c, fills):
        for stage, lag in ((first, 1), (second, 2), (third, 3)):
            if 0 <= c - lag < len(chunks):
                for j in chunks[c - lag]:
                    stage(j)
                fill(fills)

    for i in range(experts + 3):
        if i < experts:
            d_first(i)
        if 0 <= i - 1 < experts:
            d_second(i - 1)
        if 0 <= i - 2 < experts:
            d_third(i - 2)
        j = i - 3
        if j >= 0:
            if j == 0:
                for copy in loads:
                    copy.wait()
            d_last(j)
            if j % step == step - 1 or j == experts - 1:
                c = j // step
                if len(chunks[c]) == 1:
                    compute(j)
                else:
                    pl.loop(chunks[c][0], chunks[c][-1] + 1)(compute)
                for k in chunks[c]:
                    for h in range(PAIR):
                        go(core_copy(k, h, 1 - lo))
                returns(c, 1 if c == len(chunks) - 1 else 0)
    for c in range(len(chunks), len(chunks) + 3):
        returns(c, 1)
    fill(len(items))

    gain = gain_ref[...]
    saved = normed_ref[...].astype(F32)
    pre_act = saved * gain
    act_sig = jax.nn.sigmoid(pre_act)
    slope = act_sig * (1.0 + pre_act * (1.0 - act_sig))
    proj_act = (pre_act * act_sig).astype(BF16)

    stream = cot_ref[...].astype(F32)
    for j in [0] + list(range(1, experts)):
        if j:
            z_copy(j).wait_recv()
            block = back[j]
        else:
            block = done[0]
        source = lax.rem(e + j, experts)
        hot = one_hot(rank_ref[pl.ds(source, 1), :], cap).astype(BF16)
        stream = stream + dot_rows(hot, block)
    stream = stream.astype(BF16)
    stream_ref[...] = stream
    full[:, cols_of(t)] = stream

    def gather_copy(n, col, device):
        return remote(full.at[:, cols_of(col)], full.at[:, cols_of(col)], t_send.at[n], t_recv.at[n], device)

    go(gather_copy(0, t, across))
    go(gather_copy(1, t, partner))
    gather_copy(0, across[1], across).wait_recv()
    go(gather_copy(2, across[1], partner))
    gather_copy(1, partner[1], partner).wait_recv()
    gather_copy(2, far[1], partner).wait_recv()

    rows = pg.shape[2]

    def p_copy(j):
        return remote(pg.at[j, 1 - g], py.at[j], p_send.at[j], p_recv.at[j], beside)

    whole = dot_rows(full[...], proj_act)
    pall = whole.reshape(experts, GROUP, rows, whole.shape[1])
    for i in range(experts):
        pg[i] = pall[i].astype(BF16)
    for i in range(experts):
        go(p_copy(i))

    proj_in = jnp.dot(full[...], proj_ref[...], preferred_element_type=F32)
    norm_grad = proj_in * slope * gain
    one = jnp.sum(norm_grad, axis=1, keepdims=True)
    two = jnp.sum(norm_grad * saved, axis=1, keepdims=True)
    lane = lax.broadcasted_iota(jnp.int32, (tok, 128), 1)
    packed = jnp.where(lane == 0, one, jnp.where(lane == 1, two, 0.0))
    stats[t] = packed.T[:8]

    def stat_copy(n, device, owner):
        return remote(stats.at[owner], stats.at[owner], t_send.at[n], t_recv.at[n], device)

    for n, device in ((3, across), (4, far), (5, partner)):
        go(stat_copy(n, device, t))

    def q_copy(j):
        return remote(pz_out.at[j], pz.at[j], q_send.at[j], q_recv.at[j], z_peers[j - 1])

    for n, device in ((3, across), (4, far), (5, partner)):
        stat_copy(n, device, device[1]).wait_recv()
    total = stats[0]
    for i in range(1, tp_ways):
        total = total + stats[i]
    total = jnp.concatenate([total, jnp.zeros((120, tok), F32)], axis=0).T
    channels = saved.shape[1] * tp_ways
    mean_one = total[:, 0:1] / channels
    mean_two = total[:, 1:2] / channels
    conv = std_ref[...] * (norm_grad - mean_one - saved * mean_two)
    ext[pl.ds(0, tok), :] = conv

    def halo_copy():
        return remote(ext.at[pl.ds(0, 32)], ext.at[pl.ds(tok, 32)], t_send.at[6], t_recv.at[6], before)

    @pl.when(s > 0)
    def _():
        halo_copy().start()

    for i in range(experts):
        p_copy(i).wait_recv()
    for j in list(range(1, experts)) + [0]:
        target = lax.rem(e + j, experts)
        piece = pg[target, g].astype(F32) + py[target].astype(F32)
        if j:
            pz_out[j] = piece.astype(BF16)
            go(q_copy(j))
        else:
            pgrad_ref[...] = piece

    @pl.when(s < sp_ways - 1)
    def _():
        halo_copy().wait_recv()

    @pl.when(s == sp_ways - 1)
    def _():
        ext[pl.ds(tok, 32), :] = jnp.zeros((32, ext.shape[1]), F32)

    glu = taps_ref[0:1, :] * ext[pl.ds(0, tok), :]
    for k in range(1, ksize):
        glu = glu + taps_ref[k : k + 1, :] * ext[pl.ds(k, tok), :]
    in_sig = jax.nn.sigmoid(gate_ref[...].astype(F32))
    vgrad_ref[...] = (glu * in_sig).astype(BF16)
    ggrad_ref[...] = (glu * value_ref[...].astype(F32) * in_sig * (1.0 - in_sig)).astype(BF16)

    total = pgrad_ref[...]
    for j in range(1, experts):
        q_copy(j).wait_recv()
        total = total + pz[j].astype(F32)
    pgrad_ref[...] = total

    @pl.when(s > 0)
    def _():
        halo_copy().wait_send()

    for copy in sent:
        copy.wait_send()
    for copy in stores:
        copy.wait()


def mega(h_part, rank, weight, w_gate, w_up, w_down, cot, value, gate_in, normed, std, gain, taps, w_proj, experts, cap, tp_ways):
    vmem = pl.BlockSpec(memory_space=pltpu.VMEM)
    hbm = pl.BlockSpec(memory_space=pl.ANY)
    tok, quarter = cot.shape
    width, hidden = w_gate.shape
    total = experts * GROUP * cap
    ch = normed.shape[1]
    rows = width // (experts * GROUP)
    half = quarter // 2
    dma = pltpu.SemaphoreType.DMA
    assert taps.shape[0] - 1 <= 32
    return pl.pallas_call(
        functools.partial(mega_kernel, experts, cap, taps.shape[0]),
        out_shape=(
            jax.ShapeDtypeStruct((width, hidden), BF16),
            jax.ShapeDtypeStruct((width, hidden), BF16),
            jax.ShapeDtypeStruct((hidden, width), BF16),
            jax.ShapeDtypeStruct((tok, quarter), BF16),
            jax.ShapeDtypeStruct((rows, ch), F32),
            jax.ShapeDtypeStruct((tok, ch), BF16),
            jax.ShapeDtypeStruct((tok, ch), BF16),
        ),
        in_specs=[vmem] * 4 + [hbm] * 3 + [vmem] * 7,
        out_specs=(hbm,) * 3 + (vmem,) * 4,
        scratch_shapes=[
            pltpu.VMEM((2, total, width), BF16),
            pltpu.VMEM((experts, 2, cap, quarter), BF16),
            pltpu.VMEM((width, hidden), BF16),
            pltpu.VMEM((width, hidden), BF16),
            pltpu.VMEM((hidden, width), BF16),
            pltpu.VMEM((total, hidden), BF16),
            pltpu.VMEM((total, hidden), BF16),
            pltpu.VMEM((total, hidden), BF16),
            pltpu.VMEM((total, width), BF16),
            pltpu.VMEM((width, hidden), BF16),
            pltpu.VMEM((width, hidden), BF16),
            pltpu.VMEM((hidden, width), BF16),
            pltpu.VMEM((experts, PAIR, GROUP * cap, quarter), BF16),
            pltpu.VMEM((2, experts, PAIR, GROUP, cap, half), BF16),
            pltpu.VMEM((experts, GROUP, cap, half), BF16),
            pltpu.VMEM((experts, PAIR, cap, half), BF16),
            pltpu.VMEM((2, experts, cap, half), BF16),
            pltpu.VMEM((2, experts, cap, half), BF16),
            pltpu.VMEM((experts, cap, quarter), BF16),
            pltpu.VMEM((experts, cap, quarter), BF16),
            pltpu.VMEM((tok, width), BF16),
            pltpu.VMEM((tp_ways, 8, tok), F32),
            pltpu.VMEM((tok + 32, ch), F32),
            pltpu.VMEM((experts, GROUP, rows, ch), BF16),
            pltpu.VMEM((experts, rows, ch), BF16),
            pltpu.VMEM((experts, rows, ch), BF16),
            pltpu.VMEM((experts, rows, ch), BF16),
            dma((3,)),
            dma((3,)),
            dma((experts,)),
            dma((experts,)),
            dma((experts, 9)),
            dma((experts, 9)),
            dma((experts, PAIR)),
            dma((experts, PAIR)),
            dma((experts, 4)),
            dma((experts, 4)),
            dma((experts,)),
            dma((experts,)),
            dma((7,)),
            dma((7,)),
            dma((experts,)),
            dma((experts,)),
            dma((experts,)),
            dma((experts,)),
        ],
        compiler_params=pltpu.CompilerParams(
            collective_id=0, has_side_effects=True, vmem_limit_bytes=56 * 1024 * 1024
        ),
        name="mega",
    )(h_part, cot, rank, weight, w_gate, w_up, w_down, value, gate_in, normed, std, gain, taps, w_proj)


def on_device(
    hidden_state, out_grad, routes, route_weights, w_gate, w_up, w_down,
    value, gate_in, normed, inv_std, norm_gain, taps, w_proj,
):
    tok, width = hidden_state.shape
    top_k = routes.shape[1]
    sp_ways, tp_ways = lax.axis_size("sp"), lax.axis_size("tp")
    experts = sp_ways // GROUP
    cap = 3 * tok * top_k // (2 * experts)
    cap = -(-cap // 16) * 16
    quarter = width // tp_ways
    offset = lax.axis_index("tp") * quarter
    names = routes[None, :, :] == jnp.arange(experts, dtype=jnp.int32)[:, None, None]
    named = jnp.any(names, axis=2)
    weight = jnp.sum(jnp.where(names, route_weights[None], 0.0), axis=2)
    index = jnp.arange(tok)
    earlier = (index[:, None] < index[None, :]).astype(BF16)
    rank = jnp.dot(named.astype(BF16), earlier, preferred_element_type=F32).astype(jnp.int32)
    rank = jnp.where(named, rank, -1)
    h_part = lax.dynamic_slice_in_dim(hidden_state, offset, quarter, 1)
    c_part = lax.dynamic_slice_in_dim(out_grad, offset, quarter, 1)
    gate_wgrad, up_wgrad, down_grad, stream_part, proj_grad, value_grad, gate_in_grad = mega(
        h_part, rank, weight, w_gate[0], w_up[0], w_down[0], c_part, value, gate_in, normed,
        inv_std[:, None], norm_gain[None, :], taps, w_proj, experts, cap, tp_ways,
    )
    return gate_wgrad[None], up_wgrad[None], down_grad[None], stream_part, proj_grad, value_grad, gate_in_grad


def solution(mesh):
    in_specs = (
        P("sp", None), P("sp", None), P("sp", None), P("sp", None),
        P("sp", None, "tp"), P("sp", None, "tp"), P("sp", "tp", None),
        P("sp", "tp"), P("sp", "tp"), P("sp", "tp"), P("sp"), P("tp"), P(None, "tp"), P(None, "tp"),
    )
    out_specs = (
        P("sp", None, "tp"), P("sp", None, "tp"), P("sp", "tp", None),
        P("sp", "tp"), P("sp", "tp"), P("sp", "tp"), P("sp", "tp"),
    )
    return jax.shard_map(on_device, mesh=mesh, in_specs=in_specs, out_specs=out_specs, check_vma=False)
```

profile of v0, /device:TPU:0, one launch (start us, length us, event | category | flops | bytes accessed | tf_op | source)
XLA Modules:
  0.0 108.7 jit_solution(1198152891053707549)
XLA Ops:
  0.6 0.7 fusion.1
  1.3 0.7 fusion.rank_ref
  2.0 1.3 %select_reduce_fusion.w_ref = f32[4,128]{1,0:T(4,128)} fusion(f32[128,2]{0,1:T(2,128)} %param.17, s32[128,2]{0,1:T(2,128)} %param.16), kind=kLoop, calls=%fused_computation.3 | loop fusion | flops 2560 | bytes 4096 | tf_op jit(solution)/shard_map/reduce_sum | solution.py:514
  3.3 1.4 %copy.30.std_ref = f32[128,1]{1,0:T(8,128)} copy(f32[128,1]{0,1:T(1,128)} %bitcast.15) | data formatting | bytes 1024 | tf_op jit(solution)/shard_map/broadcast_in_dim | solution.py:523
  4.7 1.7 %constant_dynamic-slice_fusion = (bf16[128,512]{1,0:T(8,128)(2,1)}, bf16[128,512]{1,0:T(8,128)(2,1)}) fusion(bf16[128,2048]{1,0:T(8,128)(2,1)} %param.15, s32[]{:T(128)S(6)} %select_n.12, bf16[128,2048]{1,0:T(8,128)(2,1)} %param.14), kind=kLoop, calls=%fused_computation.6 | loop fusion | bytes 524292 | tf_op jit(solution)/shard_map/dynamic_slice | solution.py:520
  6.4 0.0 copy-start.1
  6.4 3.9 %copy.28 = bf16[1,2048,448]{2,1,0:T(8,128)(2,1)} copy(bf16[1,2048,448]{1,2,0:T(8,128)(2,1)} %param.18) | data formatting | bytes 3670016 | tf_op args[4]
  10.4 0.0 copy-done.1
  10.4 2.4 %copy.29 = bf16[1,2048,448]{2,1,0:T(8,128)(2,1)} copy(bf16[1,2048,448]{1,2,0:T(8,128)(2,1)S(1)} %copy-done.1) | data formatting | bytes 3670016 | tf_op args[5]
  12.8 84.1 %mega.1 = (bf16[2048,448]{1,0:T(8,128)(2,1)}, bf16[2048,448]{1,0:T(8,128)(2,1)}, bf16[448,2048]{1,0:T(8,128)(2,1)}, bf16[128,512]{1,0:T(8,128)(2,1)}, f32[256,12...) custom-call(bf16[128,512]{1,0:T(8,128)(2,1)} %get-tuple-element.36.h_ref, ...), custom_call_target="tpu_custom_call" | custom-call | tf_op jit(solution)/shard_map/mega/pallas_call | solution.py:433
  96.9 0.0 copy-start
  96.9 4.0 %copy.31 = bf16[1,2048,448]{1,2,0:T(8,128)(2,1)} copy(bf16[1,2048,448]{2,1,0:T(8,128)(2,1)} %bitcast.12) | data formatting | bytes 3670016
  100.9 0.0 copy-done
  100.9 2.3 %copy.32 = bf16[1,2048,448]{1,2,0:T(8,128)(2,1)} copy(bf16[1,2048,448]{2,1,0:T(8,128)(2,1)S(1)} %bitcast.11) | data formatting | bytes 3670016
  103.2 0.0 copy-start.3
  103.2 0.0 copy-start.2
  103.2 0.0 copy-start.5
  103.2 0.0 copy-start.4
  103.2 3.0 %copy.38 = bf16[1,448,2048]{2,1,0:T(8,128)(2,1)} copy(bf16[1,448,2048]{2,1,0:T(8,128)(2,1)} %bitcast.13) | data formatting | bytes 3670016
  106.2 0.0 copy-done.3
  106.2 0.7 copy.39
  106.9 0.0 copy-done.2
  106.9 0.7 copy.40
  107.5 0.0 copy-done.5
  107.5 0.6 copy.41
  108.1 0.0 copy-done.4
  108.1 0.6 copy.42
Async XLA Ops:
  6.4 4.0 %copy-start.1 = (bf16[1,2048,448]{1,2,0:T(8,128)(2,1)S(1)}, bf16[1,2048,448]{1,2,0:T(8,128)(2,1)}, u32[]{:S(2)}) copy-start(bf16[1,2048,448]{1,2,0:T(8,128)(2,1)} %param.19) | copy-start | bytes 5505028
  96.9 4.0 %copy-start = (bf16[2048,448]{1,0:T(8,128)(2,1)S(1)}, bf16[2048,448]{1,0:T(8,128)(2,1)}, u32[]{:S(2)}) copy-start(bf16[2048,448]{1,0:T(8,128)(2,1)} %get-tuple-element.15) | copy-start | bytes 5505028
  103.2 3.0 %copy-start.3 = (bf16[128,512]{1,0:T(8,128)(2,1)S(1)}, bf16[128,512]{1,0:T(8,128)(2,1)}, u32[]{:S(2)}) copy-start(bf16[128,512]{1,0:T(8,128)(2,1)} %get-tuple-element.47) | copy-start | bytes 393220
  103.2 3.7 %copy-start.2 = (f32[256,128]{1,0:T(8,128)S(1)}, f32[256,128]{1,0:T(8,128)}, u32[]{:S(2)}) copy-start(f32[256,128]{1,0:T(8,128)} %get-tuple-element.48) | copy-start | bytes 393220
  103.2 4.3 %copy-start.5 = (bf16[128,128]{1,0:T(8,128)(2,1)S(1)}, bf16[128,128]{1,0:T(8,128)(2,1)}, u32[]{:S(2)}) copy-start(bf16[128,128]{1,0:T(8,128)(2,1)} %get-tuple-element.49) | copy-start | bytes 98308
  103.2 4.9 %copy-start.4 = (bf16[128,128]{1,0:T(8,128)(2,1)S(1)}, bf16[128,128]{1,0:T(8,128)(2,1)}, u32[]{:S(2)}) copy-start(bf16[128,128]{1,0:T(8,128)(2,1)} %get-tuple-element.50) | copy-start | bytes 98308
where the time goes:
time: 109 us
  Pallas kernels  84.1 us (77%)
  local copies, waits for them, and re-layouts  21.3 us (20%)
  other arithmetic  1.98 us (2%)
    pallas_call x1, Pallas kernels, mega(): pl.pallas_call(functools.partial(mega_kernel, experts, cap, taps.shape[0]...  84.1 us
    unnamed x21, local copies, waits for them, and re-layouts  18.2 us

commit v1 on v0

--- a/solution.py
+++ b/solution.py
@@ -50,14 +50,32 @@
     return jnp.where(slots == rank_row, 1.0, 0.0)
 
 
+def rank_tokens(routes_ref, weights_ref, rank_ref, w_ref):
+    top, tok = routes_ref.shape
+    experts = lax.broadcasted_iota(jnp.int32, rank_ref.shape, 0)
+    named = jnp.zeros(rank_ref.shape, F32)
+    weight = jnp.zeros(rank_ref.shape, F32)
+    for k in range(top):
+        hit = routes_ref[k : k + 1, :] == experts
+        named = jnp.where(hit, 1.0, named)
+        weight = jnp.where(hit, weights_ref[k : k + 1, :], weight)
+    first = lax.broadcasted_iota(jnp.int32, (tok, tok), 0)
+    second = lax.broadcasted_iota(jnp.int32, (tok, tok), 1)
+    earlier = jnp.where(first < second, 1.0, 0.0).astype(BF16)
+    rank = jnp.dot(named.astype(BF16), earlier, preferred_element_type=F32)
+    rank_ref[...] = jnp.where(named > 0.0, rank, -1.0).astype(jnp.int32)
+    w_ref[...] = weight
+
+
 def mega_kernel(
     experts, cap, ksize,
-    h_ref, cot_ref, rank_ref, w_ref, gate_hbm, up_hbm, down_hbm,
-    value_ref, gate_ref, normed_ref, std_ref, gain_ref, taps_ref, proj_ref,
-    gw_hbm, uw_hbm, dw_hbm, stream_ref, pgrad_ref, vgrad_ref, ggrad_ref,
-    buf, pack, wg, wu, wd, act, gg, ug, grad_ref, gw, uw, dw,
+    h_hbm, cot_hbm, routes_hbm, weights_hbm, gate_hbm, up_hbm, down_hbm,
+    value_hbm, gin_hbm, normed_hbm, std_hbm, gain_hbm, taps_hbm, proj_hbm,
+    gw, uw, dw, stream_ref, pgrad_ref, vgrad_ref, ggrad_ref,
+    h_ref, cot_ref, routes_ref, weights_ref, value_ref, gate_ref, normed_ref, std_ref, gain_ref, taps_ref, proj_ref,
+    rank_ref, w_ref, buf, pack, wg, wu, wd, act, gg, ug, flipped, grad_ref,
     from_core, sums, rx_a, ry_b, relay, rx2, back, done, full, stats, ext, pg, py, pz_out, pz,
-    w_sem, o_sem, d_send, d_recv, g_send, g_recv,
+    h_sem, w_sem, x_sem, d_send, d_recv, g_send, g_recv,
     core_send, core_recv, hop_send, hop_recv, z_send, z_recv, t_send, t_recv, p_send, p_recv, q_send, q_recv,
 ):
     s, t, e, g, hi, lo, across, beside, partner = place()
@@ -71,12 +89,27 @@
     z_peers = [(lax.rem(e + j, experts) * GROUP + g, t) for j in range(1, experts)]
     before = (lax.rem(s + sp_ways - 1, sp_ways), t)
     after = (lax.rem(s + 1, sp_ways), t)
-    loads = [
-        pltpu.make_async_copy(src, dst, w_sem.at[n])
-        for n, (src, dst) in enumerate(((gate_hbm, wg), (up_hbm, wu), (down_hbm, wd)))
-    ]
-    for copy in loads:
+    cut = pl.ds(pl.multiple_of(t * quarter, quarter), quarter)
+
+    def fetch(sem, *pairs):
+        return [pltpu.make_async_copy(src, dst, sem.at[n]) for n, (src, dst) in enumerate(pairs)]
+
+    takes = fetch(
+        h_sem, (routes_hbm, routes_ref), (weights_hbm, weights_ref),
+        (h_hbm.at[:, cut], h_ref), (cot_hbm.at[:, cut], cot_ref),
+    )
+    loads = fetch(w_sem, (gate_hbm, wg), (up_hbm, wu), (down_hbm, wd))
+    extras = fetch(
+        x_sem, (normed_hbm, normed_ref), (gain_hbm, gain_ref), (proj_hbm, proj_ref), (std_hbm, std_ref),
+        (taps_hbm, taps_ref), (gin_hbm, gate_ref), (value_hbm, value_ref),
+    )
+    for copy in takes + loads + extras:
         copy.start()
+    for copy in takes[:2]:
+        copy.wait()
+    rank_tokens(routes_ref, weights_ref, rank_ref, w_ref)
+    for copy in takes[2:]:
+        copy.wait()
     sent = []
 
     def go(copy):
@@ -90,15 +123,14 @@
         return lax.rem(e + experts - j, experts)
 
     def rows_of(j):
-        return pl.ds(pl.multiple_of(source_of(j) * GROUP * cap, cap), GROUP * cap)
+        return pl.ds(pl.multiple_of(j * GROUP * cap, cap), GROUP * cap)
 
     def loc(j, side, col):
-        return pl.ds(pl.multiple_of((source_of(j) * GROUP + side) * cap, cap), cap), cols_of(col)
-
-    own_rows, own_cols = loc(0, g, t)
+        return pl.ds(pl.multiple_of((j * GROUP + side) * cap, cap), cap), cols_of(col)
 
     def d_copy(j):
-        return remote(pack.at[j], buf.at[:, own_rows, own_cols], d_send.at[j], d_recv.at[j], z_peers[j - 1])
+        there, cols = loc(j, g, t)
+        return remote(pack.at[j], buf.at[:, there, cols], d_send.at[j], d_recv.at[j], z_peers[j - 1])
 
     greeted = False
     for j in list(range(1, experts)) + [0]:
@@ -116,8 +148,9 @@
                 greeted = True
             go(d_copy(j))
         else:
-            buf[0, own_rows, own_cols] = rows
-            buf[1, own_rows, own_cols] = cots
+            here, cols = loc(0, g, t)
+            buf[0, here, cols] = rows
+            buf[1, here, cols] = cots
 
     def hop(n, j, ref, device):
         return remote(ref, ref, g_send.at[j, n], g_recv.at[j, n], device)
@@ -166,8 +199,8 @@
         rows = rows_of(j)
         in_rows = buf[0, rows, :]
         in_cots = buf[1, rows, :]
-        pre_gate = jnp.dot(in_rows, wg[...], preferred_element_type=F32)
-        pre_up = jnp.dot(in_rows, wu[...], preferred_element_type=F32)
+        pre_gate = dot_cols(in_rows, wg[...])
+        pre_up = dot_cols(in_rows, wu[...])
         gate_sig = jax.nn.sigmoid(pre_gate)
         silu_gate = pre_gate * gate_sig
         act_grad = dot_cols(in_cots, wd[...])
@@ -176,27 +209,24 @@
         act[rows, :] = (silu_gate * pre_up).astype(BF16)
         gg[rows, :] = gate_grad
         ug[rows, :] = up_grad
-        grad_ref[rows, :] = (dot_cols(gate_grad, wg[...]) + dot_cols(up_grad, wu[...])).astype(BF16)
+        grad_ref[rows, :] = (
+            jnp.dot(gate_grad, wg[...], preferred_element_type=F32) + jnp.dot(up_grad, wu[...], preferred_element_type=F32)
+        ).astype(BF16)
 
     width = full.shape[1]
     piece = 256
     per_item = width // piece // 4
 
     def weight_item(which, n):
+        if n == 0:
+            flipped[...] = (gg, ug, act)[which][...].T
+
         @pl.loop(n * per_item, (n + 1) * per_item)
         def _(i):
             cols = pl.ds(pl.multiple_of(i * piece, piece), piece)
-            if which == 0:
-                gw[cols, :] = dot_rows(buf[0, :, cols], gg[...]).astype(BF16)
-            elif which == 1:
-                uw[cols, :] = dot_rows(buf[0, :, cols], ug[...]).astype(BF16)
-            else:
-                dw[:, cols] = dot_rows(act[...], buf[1, :, cols]).astype(BF16)
-
-    stores = [
-        pltpu.make_async_copy(src, dst, o_sem.at[n])
-        for n, (src, dst) in enumerate(((gw, gw_hbm), (uw, uw_hbm), (dw, dw_hbm)))
-    ]
+            rows = buf[1 if which == 2 else 0, :, cols]
+            (gw, uw, dw)[which][:, cols] = jnp.dot(flipped[...], rows, preferred_element_type=F32).astype(BF16)
+
     items = [(which, n) for which in range(3) for n in range(4)]
 
     def fill(count=1):
@@ -204,8 +234,6 @@
             if items:
                 which, n = items.pop(0)
                 weight_item(which, n)
-                if n == 3:
-                    stores[which].start()
 
     def core_copy(j, h, lane):
         return remote(
@@ -298,6 +326,8 @@
         returns(c, 1)
     fill(len(items))
 
+    for copy in extras:
+        copy.wait()
     gain = gain_ref[...]
     saved = normed_ref[...].astype(F32)
     pre_act = saved * gain
@@ -367,7 +397,8 @@
     channels = saved.shape[1] * tp_ways
     mean_one = total[:, 0:1] / channels
     mean_two = total[:, 1:2] / channels
-    conv = std_ref[...] * (norm_grad - mean_one - saved * mean_two)
+    std = jnp.broadcast_to(std_ref[...], (tok, tok)).T[:, 0:1]
+    conv = std * (norm_grad - mean_one - saved * mean_two)
     ext[pl.ds(0, tok), :] = conv
 
     def halo_copy():
@@ -415,47 +446,51 @@
 
     for copy in sent:
         copy.wait_send()
-    for copy in stores:
-        copy.wait()
-
-
-def mega(h_part, rank, weight, w_gate, w_up, w_down, cot, value, gate_in, normed, std, gain, taps, w_proj, experts, cap, tp_ways):
+
+
+def mega(hidden, cot, routes, weights, w_gate, w_up, w_down, value, gate_in, normed, std, gain, taps, w_proj, experts, cap, tp_ways):
     vmem = pl.BlockSpec(memory_space=pltpu.VMEM)
     hbm = pl.BlockSpec(memory_space=pl.ANY)
-    tok, quarter = cot.shape
-    width, hidden = w_gate.shape
+    tok, width = cot.shape
+    units = w_gate.shape[0]
+    quarter = width // tp_ways
+    padded = -(-experts // 8) * 8
     total = experts * GROUP * cap
     ch = normed.shape[1]
     rows = width // (experts * GROUP)
     half = quarter // 2
     dma = pltpu.SemaphoreType.DMA
+    arrays = (hidden, cot, routes, weights, w_gate, w_up, w_down, value, gate_in, normed, std, gain, taps, w_proj)
     assert taps.shape[0] - 1 <= 32
     return pl.pallas_call(
         functools.partial(mega_kernel, experts, cap, taps.shape[0]),
         out_shape=(
-            jax.ShapeDtypeStruct((width, hidden), BF16),
-            jax.ShapeDtypeStruct((width, hidden), BF16),
-            jax.ShapeDtypeStruct((hidden, width), BF16),
-            jax.ShapeDtypeStruct((tok, quarter), BF16),
-            jax.ShapeDtypeStruct((rows, ch), F32),
-            jax.ShapeDtypeStruct((tok, ch), BF16),
-            jax.ShapeDtypeStruct((tok, ch), BF16),
+            pltpu.VMEM((units, width), BF16),
+            pltpu.VMEM((units, width), BF16),
+            pltpu.VMEM((units, width), BF16),
+            pltpu.VMEM((tok, quarter), BF16),
+            pltpu.VMEM((rows, ch), F32),
+            pltpu.VMEM((tok, ch), BF16),
+            pltpu.VMEM((tok, ch), BF16),
         ),
-        in_specs=[vmem] * 4 + [hbm] * 3 + [vmem] * 7,
-        out_specs=(hbm,) * 3 + (vmem,) * 4,
+        in_specs=[hbm] * len(arrays),
+        out_specs=(vmem,) * 7,
         scratch_shapes=[
+            pltpu.VMEM((tok, quarter), BF16),
+            pltpu.VMEM((tok, quarter), BF16),
+            *[pltpu.VMEM(a.shape, a.dtype) for a in (routes, weights, value, gate_in, normed, std, gain, taps, w_proj)],
+            pltpu.VMEM((padded, tok), jnp.int32),
+            pltpu.VMEM((padded, tok), F32),
             pltpu.VMEM((2, total, width), BF16),
             pltpu.VMEM((experts, 2, cap, quarter), BF16),
-            pltpu.VMEM((width, hidden), BF16),
-            pltpu.VMEM((width, hidden), BF16),
-            pltpu.VMEM((hidden, width), BF16),
-            pltpu.VMEM((total, hidden), BF16),
-            pltpu.VMEM((total, hidden), BF16),
-            pltpu.VMEM((total, hidden), BF16),
+            pltpu.VMEM((units, width), BF16),
+            pltpu.VMEM((units, width), BF16),
+            pltpu.VMEM((units, width), BF16),
+            pltpu.VMEM((total, units), BF16),
+            pltpu.VMEM((total, units), BF16),
+            pltpu.VMEM((total, units), BF16),
+            pltpu.VMEM((units, total), BF16),
             pltpu.VMEM((total, width), BF16),
-            pltpu.VMEM((width, hidden), BF16),
-            pltpu.VMEM((width, hidden), BF16),
-            pltpu.VMEM((hidden, width), BF16),
             pltpu.VMEM((experts, PAIR, GROUP * cap, quarter), BF16),
             pltpu.VMEM((2, experts, PAIR, GROUP, cap, half), BF16),
             pltpu.VMEM((experts, GROUP, cap, half), BF16),
@@ -471,8 +506,9 @@
             pltpu.VMEM((experts, rows, ch), BF16),
             pltpu.VMEM((experts, rows, ch), BF16),
             pltpu.VMEM((experts, rows, ch), BF16),
+            dma((4,)),
             dma((3,)),
-            dma((3,)),
+            dma((7,)),
             dma((experts,)),
             dma((experts,)),
             dma((experts, 9)),
@@ -491,38 +527,49 @@
             dma((experts,)),
         ],
         compiler_params=pltpu.CompilerParams(
-            collective_id=0, has_side_effects=True, vmem_limit_bytes=56 * 1024 * 1024
+            collective_id=0, has_side_effects=True, vmem_limit_bytes=44 * 1024 * 1024
         ),
         name="mega",
-    )(h_part, cot, rank, weight, w_gate, w_up, w_down, value, gate_in, normed, std, gain, taps, w_proj)
+    )(*[pltpu.with_memory_space_constraint(a, pltpu.HBM) for a in arrays])
+
+
+def finish_kernel(count, *refs):
+    copies = [pltpu.make_async_copy(refs[n], refs[count + n], refs[-1].at[n]) for n in range(count)]
+    for copy in copies:
+        copy.start()
+    for copy in copies:
+        copy.wait()
+
+
+def finish(*arrays):
+    count = len(arrays)
+    return pl.pallas_call(
+        functools.partial(finish_kernel, count),
+        out_shape=tuple(jax.ShapeDtypeStruct(a.shape, a.dtype) for a in arrays),
+        in_specs=[pl.BlockSpec(memory_space=pltpu.VMEM)] * count,
+        out_specs=(pl.BlockSpec(memory_space=pl.ANY),) * count,
+        scratch_shapes=[pltpu.SemaphoreType.DMA((count,))],
+        compiler_params=pltpu.CompilerParams(vmem_limit_bytes=8 * 1024 * 1024),
+        name="finish",
+    )(*[pltpu.with_memory_space_constraint(a, pltpu.VMEM) for a in arrays])
 
 
 def on_device(
     hidden_state, out_grad, routes, route_weights, w_gate, w_up, w_down,
     value, gate_in, normed, inv_std, norm_gain, taps, w_proj,
 ):
-    tok, width = hidden_state.shape
+    tok = hidden_state.shape[0]
     top_k = routes.shape[1]
     sp_ways, tp_ways = lax.axis_size("sp"), lax.axis_size("tp")
     experts = sp_ways // GROUP
     cap = 3 * tok * top_k // (2 * experts)
     cap = -(-cap // 16) * 16
-    quarter = width // tp_ways
-    offset = lax.axis_index("tp") * quarter
-    names = routes[None, :, :] == jnp.arange(experts, dtype=jnp.int32)[:, None, None]
-    named = jnp.any(names, axis=2)
-    weight = jnp.sum(jnp.where(names, route_weights[None], 0.0), axis=2)
-    index = jnp.arange(tok)
-    earlier = (index[:, None] < index[None, :]).astype(BF16)
-    rank = jnp.dot(named.astype(BF16), earlier, preferred_element_type=F32).astype(jnp.int32)
-    rank = jnp.where(named, rank, -1)
-    h_part = lax.dynamic_slice_in_dim(hidden_state, offset, quarter, 1)
-    c_part = lax.dynamic_slice_in_dim(out_grad, offset, quarter, 1)
-    gate_wgrad, up_wgrad, down_grad, stream_part, proj_grad, value_grad, gate_in_grad = mega(
-        h_part, rank, weight, w_gate[0], w_up[0], w_down[0], c_part, value, gate_in, normed,
-        inv_std[:, None], norm_gain[None, :], taps, w_proj, experts, cap, tp_ways,
+    results = mega(
+        hidden_state, out_grad, routes.T, route_weights.T, w_gate[0].T, w_up[0].T, w_down[0], value, gate_in, normed,
+        inv_std[None, :], norm_gain[None, :], taps, w_proj, experts, cap, tp_ways,
     )
-    return gate_wgrad[None], up_wgrad[None], down_grad[None], stream_part, proj_grad, value_grad, gate_in_grad
+    gate_wgrad, up_wgrad, down_grad, stream_part, proj_grad, value_grad, gate_in_grad = finish(*results)
+    return gate_wgrad.T[None], up_wgrad.T[None], down_grad[None], stream_part, proj_grad, value_grad, gate_in_grad
 
 
 def solution(mesh):

time: 109 us -> 88.1 us (0.81)
  local copies, waits for them, and re-layouts: 21.3 us -> 0 us
  Pallas kernels: 84.1 us -> 87.2 us
  other arithmetic: 1.98 us -> 0 us
    unnamed x21 -> x0, local copies, waits for them, and re-layouts: 18.2 us -> none
    pallas_call x0 -> x1, Pallas kernels: none -> 2.58 us  [finish(): pl.pallas_call(functools.partial(finish_kernel, count), out_shape=tuple((...]
    dynamic_slice x1 -> x0, local copies, waits for them, and re-layouts: 1.68 us -> none  [on_device(): c_part = lax.dynamic_slice_in_dim(out_grad, offset, quarter, 1)]
    broadcast_in_dim x1 -> x0, local copies, waits for them, and re-layouts: 1.39 us -> none  [on_device(): inv_std[:, None]]
    reduce_sum x1 -> x0, other arithmetic: 1.28 us -> none  [on_device(): weight = jnp.sum(jnp.where(names, route_weights[None], 0.0), axis=2)]
where the time goes in v1:
time: 88.1 us; the launch traced here: 88 us
  Pallas kernels  87.2 us (99%)
    pallas_call x1, Pallas kernels, mega(): pl.pallas_call(functools.partial(mega_kernel, experts, cap, taps.shape[0]...  84.6 us
    pallas_call x1, Pallas kernels, finish(): pl.pallas_call(functools.partial(finish_kernel, count), out_shape=tuple((...  2.58 us

profile of v1, /device:TPU:0, one launch (start us, length us, event | category | flops | bytes accessed | tf_op | source)
XLA Modules:
  0.0 88.0 jit_solution(18200658168738223231)
XLA Ops:
  0.6 84.6 %mega.1 = (bf16[448,2048]{1,0:T(8,128)(2,1)S(1)}, bf16[448,2048]{1,0:T(8,128)(2,1)S(1)}, bf16[448,2048]{1,0:T(8,128)(2,1)S(1)}, bf16[128,512]{1,0:T(8,128)(2,1)S...) custom-call(bf16[128,2048]{1,0:T(8,128)(2,1)} %h_hbm.1, ...), custom_call_target="tpu_custom_call" | custom-call | tf_op jit(solution)/shard_map/mega/pallas_call | solution.py:465
  85.3 2.6 %finish.1 = (bf16[448,2048]{1,0:T(8,128)(2,1)}, bf16[448,2048]{1,0:T(8,128)(2,1)}, bf16[448,2048]{1,0:T(8,128)(2,1)}, bf16[128,512]{1,0:T(8,128)(2,1)}, f32[256,...) custom-call(bf16[448,2048]{1,0:T(8,128)(2,1)S(1)} %get-tuple-element.21.refs_0_, ...), custom_call_target="tpu_custom_call" | custom-call | tf_op jit(solution)/shard_map/finish/pallas_call | solution.py:546

commit v2 on v1

--- a/solution.py
+++ b/solution.py
@@ -30,6 +30,15 @@
     beside = (e * GROUP + 1 - g, t)
     partner = (s, hi * PAIR + 1 - lo)
     return s, t, e, g, hi, lo, across, beside, partner
+
+
+def flip(place, bits):
+    bit = 1
+    while bit <= bits:
+        if bits & bit:
+            place = place + bit - 2 * bit * lax.rem(place // bit, 2)
+        bit *= 2
+    return place
 
 
 def greet(devices):
@@ -75,41 +84,42 @@
     h_ref, cot_ref, routes_ref, weights_ref, value_ref, gate_ref, normed_ref, std_ref, gain_ref, taps_ref, proj_ref,
     rank_ref, w_ref, buf, pack, wg, wu, wd, act, gg, ug, flipped, grad_ref,
     from_core, sums, rx_a, ry_b, relay, rx2, back, done, full, stats, ext, pg, py, pz_out, pz,
-    h_sem, w_sem, x_sem, d_send, d_recv, g_send, g_recv,
+    h_sem, w_sem, x_sem, l_send, l_recv, c_send, c_recv,
     core_send, core_recv, hop_send, hop_recv, z_send, z_recv, t_send, t_recv, p_send, p_recv, q_send, q_recv,
 ):
     s, t, e, g, hi, lo, across, beside, partner = place()
     sp_ways = experts * GROUP
-    tok, quarter = cot_ref.shape
+    tp_ways = stats.shape[0]
+    tok, quarter = cot_ref.shape[0], cot_ref.shape[1] // tp_ways
     half = quarter // 2
-    tp_ways = stats.shape[0]
     across_t, other_t = across[1], partner[1]
     far_t = (1 - hi) * PAIR + 1 - lo
     far = (s, far_t)
-    z_peers = [(lax.rem(e + j, experts) * GROUP + g, t) for j in range(1, experts)]
+    planes = [flip(e, j) for j in range(experts)]
+    z_peers = [(planes[j] * GROUP + g, t) for j in range(1, experts)]
     before = (lax.rem(s + sp_ways - 1, sp_ways), t)
     after = (lax.rem(s + 1, sp_ways), t)
-    cut = pl.ds(pl.multiple_of(t * quarter, quarter), quarter)
-
     def fetch(sem, *pairs):
         return [pltpu.make_async_copy(src, dst, sem.at[n]) for n, (src, dst) in enumerate(pairs)]
 
     takes = fetch(
         h_sem, (routes_hbm, routes_ref), (weights_hbm, weights_ref),
-        (h_hbm.at[:, cut], h_ref), (cot_hbm.at[:, cut], cot_ref),
+        (h_hbm, h_ref), (cot_hbm, cot_ref),
     )
     loads = fetch(w_sem, (gate_hbm, wg), (up_hbm, wu), (down_hbm, wd))
     extras = fetch(
         x_sem, (normed_hbm, normed_ref), (gain_hbm, gain_ref), (proj_hbm, proj_ref), (std_hbm, std_ref),
         (taps_hbm, taps_ref), (gin_hbm, gate_ref), (value_hbm, value_ref),
     )
-    for copy in takes + loads + extras:
+    for copy in takes:
         copy.start()
     for copy in takes[:2]:
         copy.wait()
     rank_tokens(routes_ref, weights_ref, rank_ref, w_ref)
     for copy in takes[2:]:
         copy.wait()
+    for copy in loads + extras:
+        copy.start()
     sent = []
 
     def go(copy):
@@ -119,81 +129,95 @@
     def cols_of(col):
         return pl.ds(pl.multiple_of(col * quarter, quarter), quarter)
 
-    def source_of(j):
-        return lax.rem(e + experts - j, experts)
-
     def rows_of(j):
         return pl.ds(pl.multiple_of(j * GROUP * cap, cap), GROUP * cap)
 
     def loc(j, side, col):
         return pl.ds(pl.multiple_of((j * GROUP + side) * cap, cap), cap), cols_of(col)
 
-    def d_copy(j):
-        there, cols = loc(j, g, t)
-        return remote(pack.at[j], buf.at[:, there, cols], d_send.at[j], d_recv.at[j], z_peers[j - 1])
-
-    greeted = False
-    for j in list(range(1, experts)) + [0]:
-        target = lax.rem(e + j, experts)
-        hot = one_hot(rank_ref[pl.ds(target, 1), :], cap)
-        scale = jnp.sum(hot * w_ref[pl.ds(target, 1), :], axis=1, keepdims=True)
-        hot = hot.astype(BF16)
-        rows = jnp.dot(hot, h_ref[...], preferred_element_type=F32).astype(BF16)
-        cots = (jnp.dot(hot, cot_ref[...], preferred_element_type=F32) * scale).astype(BF16)
+    def chosen(j):
+        plane = pl.ds(planes[j], 1)
+        hot = one_hot(rank_ref[plane, :], cap)
+        return hot.astype(BF16), jnp.sum(hot * w_ref[plane, :], axis=1, keepdims=True)
+
+    sides = (g, 1 - g)
+    spread = (t, across_t)
+
+    def spot(k, j, side, col):
+        rows, cols = loc(j, sides[side], spread[col])
+        return buf.at[k, rows, cols]
+
+    def link(k, j, side, col, src, dst, device):
+        return remote(src, dst, l_send.at[j, k, side, col], l_recv.at[j, k, side, col], device)
+
+    def landed(k, j, side, col):
+        ref = spot(k, j, side, col)
+        link(k, j, side, col, ref, ref, partner).wait_recv()
+
+    def pass_on(k, j, side, col, src, device):
+        ref = spot(k, j, *src)
+        go(link(k, j, side, col, ref, ref, device))
+
+    def core(j, side, col):
+        rows, cols = loc(j, sides[side], spread[col])
+        ref = buf.at[:, rows, cols]
+        return remote(ref, ref, c_send.at[j, side, col], c_recv.at[j, side, col], partner)
+
+    def core_landed(j, side, col):
+        rows, cols = loc(j, sides[side], (other_t, far_t)[col])
+        ref = buf.at[:, rows, cols]
+        remote(ref, ref, c_send.at[j, side, col], c_recv.at[j, side, col], partner).wait_recv()
+
+    step = max(1, experts // 4)
+    blocks = [list(range(c, min(c + step, experts))) for c in range(0, experts, step)]
+    first_block, last_blocks = blocks[1], blocks[:1:-1]
+    outer = [j for block in [first_block] + last_blocks + blocks[:1] for j in block if j]
+    for n, j in enumerate(outer):
+        hot, scale = chosen(j)
+        pack[j, 0] = jnp.dot(hot, h_ref[:, cols_of(t)], preferred_element_type=F32).astype(BF16)
+        pack[j, 1] = (jnp.dot(hot, cot_ref[:, cols_of(t)], preferred_element_type=F32) * scale).astype(BF16)
+        if not n:
+            greet(z_peers + [across, beside, partner, far, before, after])
+        for k in range(2):
+            go(link(k, j, 0, 0, pack.at[j, k], spot(k, j, 0, 0), z_peers[j - 1]))
+    hot, scale = chosen(0)
+    here = loc(0, g, t)[0]
+    buf[0, here, :] = jnp.dot(hot, h_ref[...], preferred_element_type=F32).astype(BF16)
+    buf[1, here, :] = (jnp.dot(hot, cot_ref[...], preferred_element_type=F32) * scale).astype(BF16)
+
+    def d_first(j):
+        for k in range(2):
+            if j:
+                landed(k, j, 0, 0)
+                pass_on(k, j, 0, 1, (0, 0), across)
+            pass_on(k, j, 1, 0, (0, 0), beside)
         if j:
-            pack[j, 0] = rows
-            pack[j, 1] = cots
-            if not greeted:
-                greet(z_peers + [across, beside, partner, far, before, after])
-                greeted = True
-            go(d_copy(j))
+            go(core(j, 0, 0))
+
+    def d_second(j):
+        if j:
+            landed(0, j, 0, 1)
+            pass_on(0, j, 1, 1, (0, 1), beside)
+            landed(1, j, 1, 0)
+            pass_on(1, j, 1, 1, (1, 0), across)
+            landed(1, j, 0, 1)
+            go(core(j, 0, 1))
+            landed(0, j, 1, 0)
         else:
-            here, cols = loc(0, g, t)
-            buf[0, here, cols] = rows
-            buf[1, here, cols] = cots
-
-    def hop(n, j, ref, device):
-        return remote(ref, ref, g_send.at[j, n], g_recv.at[j, n], device)
-
-    def both(j, side, col):
-        rows, cols = loc(j, side, col)
-        return buf.at[:, rows, cols]
-
-    def one_of(k, j, side, col):
-        rows, cols = loc(j, side, col)
-        return buf.at[k, rows, cols]
-
-    def arrived(n, j, ref):
-        hop(n, j, ref, partner).wait_recv()
-
-    def d_first(j):
-        block = both(j, g, t)
-        if j:
-            remote(block, block, d_send.at[j], d_recv.at[j], partner).wait_recv()
-        go(hop(0, j, block, across))
-        go(hop(1, j, block, beside))
-        go(hop(2, j, block, partner))
-
-    def d_second(j):
-        arrived(0, j, both(j, g, across_t))
-        go(hop(3, j, one_of(0, j, g, across_t), beside))
-        go(hop(5, j, both(j, g, across_t), partner))
-        arrived(1, j, both(j, 1 - g, t))
-        go(hop(4, j, one_of(1, j, 1 - g, t), across))
-        go(hop(6, j, both(j, 1 - g, t), partner))
+            for k in range(2):
+                landed(k, j, 1, 0)
+                pass_on(k, j, 1, 1, (1, 0), across)
+        go(core(j, 1, 0))
 
     def d_third(j):
-        arrived(3, j, one_of(0, j, 1 - g, across_t))
-        go(hop(7, j, one_of(0, j, 1 - g, across_t), partner))
-        arrived(4, j, one_of(1, j, 1 - g, across_t))
-        go(hop(8, j, one_of(1, j, 1 - g, across_t), partner))
+        for k in range(2):
+            landed(k, j, 1, 1)
+        go(core(j, 1, 1))
 
     def d_last(j):
-        arrived(2, j, both(j, g, other_t))
-        arrived(5, j, both(j, g, far_t))
-        arrived(6, j, both(j, 1 - g, other_t))
-        arrived(7, j, one_of(0, j, 1 - g, far_t))
-        arrived(8, j, one_of(1, j, 1 - g, far_t))
+        for side in range(0 if j else 1, 2):
+            for col in range(2):
+                core_landed(j, side, col)
 
     def compute(j):
         rows = rows_of(j)
@@ -209,9 +233,15 @@
         act[rows, :] = (silu_gate * pre_up).astype(BF16)
         gg[rows, :] = gate_grad
         ug[rows, :] = up_grad
-        grad_ref[rows, :] = (
-            jnp.dot(gate_grad, wg[...], preferred_element_type=F32) + jnp.dot(up_grad, wu[...], preferred_element_type=F32)
-        ).astype(BF16)
+        for lane in (1 - lo, lo):
+            for h in range(PAIR):
+                cols = cols_of(h * PAIR + lane)
+                grad_ref[rows, cols] = (
+                    jnp.dot(gate_grad, wg[:, cols], preferred_element_type=F32)
+                    + jnp.dot(up_grad, wu[:, cols], preferred_element_type=F32)
+                ).astype(BF16)
+                if lane is not lo and isinstance(j, int):
+                    go(core_copy(j, h, 1 - lo))
 
     width = full.shape[1]
     piece = 256
@@ -257,7 +287,7 @@
         return hop_copy(3, j, relay.at[1, j], rx2.at[1, j], across)
 
     def z_copy(j):
-        return remote(done.at[j], back.at[j], z_send.at[j], z_recv.at[j], (source_of(j) * GROUP + g, t))
+        return remote(done.at[j], back.at[j], z_send.at[j], z_recv.at[j], z_peers[j - 1])
 
     def first(j):
         for h in range(PAIR):
@@ -289,41 +319,46 @@
         if j:
             go(z_copy(j))
 
-    step = max(1, experts // 4)
-    chunks = [list(range(c, min(c + step, experts))) for c in range(0, experts, step)]
-
-    def returns(c, fills):
-        for stage, lag in ((first, 1), (second, 2), (third, 3)):
-            if 0 <= c - lag < len(chunks):
-                for j in chunks[c - lag]:
-                    stage(j)
-                fill(fills)
-
-    for i in range(experts + 3):
-        if i < experts:
-            d_first(i)
-        if 0 <= i - 1 < experts:
-            d_second(i - 1)
-        if 0 <= i - 2 < experts:
-            d_third(i - 2)
-        j = i - 3
-        if j >= 0:
-            if j == 0:
-                for copy in loads:
-                    copy.wait()
-            d_last(j)
-            if j % step == step - 1 or j == experts - 1:
-                c = j // step
-                if len(chunks[c]) == 1:
-                    compute(j)
-                else:
-                    pl.loop(chunks[c][0], chunks[c][-1] + 1)(compute)
-                for k in chunks[c]:
-                    for h in range(PAIR):
-                        go(core_copy(k, h, 1 - lo))
-                returns(c, 1 if c == len(chunks) - 1 else 0)
-    for c in range(len(chunks), len(chunks) + 3):
-        returns(c, 1)
+    def flow(*stages):
+        for stage, block in stages:
+            for j in block:
+                stage(j)
+
+    def work(block):
+        if len(block) == 1:
+            compute(block[0])
+            return
+        pl.loop(block[0], block[-1] + 1)(compute)
+        for j in block:
+            for h in range(PAIR):
+                go(core_copy(j, h, 1 - lo))
+
+    own, near, far_one, far_two = blocks[0], first_block, *last_blocks
+    d_first(0)
+    flow((d_first, near), (d_second, near), (d_first, own[1:]), (d_second, own), (d_third, near))
+    flow((d_last, near), (d_first, far_one))
+    for copy in loads:
+        copy.wait()
+    work(near)
+    flow((d_third, own), (d_first, far_two), (d_last, own))
+    work(own)
+    flow((d_second, far_one), (d_second, far_two), (first, near), (first, own), (d_third, far_one), (d_last, far_one))
+    work(far_one)
+    flow((d_third, far_two), (first, far_one), (d_last, far_two), (second, near), (second, own))
+    work(far_two)
+    flow((first, far_two))
+    fill(1)
+    flow((second, far_one))
+    fill(1)
+    flow((third, near))
+    fill(1)
+    flow((third, own))
+    fill(1)
+    flow((second, far_two))
+    fill(2)
+    flow((third, far_one))
+    fill(1)
+    flow((third, far_two))
     fill(len(items))
 
     for copy in extras:
@@ -335,15 +370,14 @@
     slope = act_sig * (1.0 + pre_act * (1.0 - act_sig))
     proj_act = (pre_act * act_sig).astype(BF16)
 
-    stream = cot_ref[...].astype(F32)
+    stream = cot_ref[:, cols_of(t)].astype(F32)
     for j in [0] + list(range(1, experts)):
         if j:
             z_copy(j).wait_recv()
             block = back[j]
         else:
             block = done[0]
-        source = lax.rem(e + j, experts)
-        hot = one_hot(rank_ref[pl.ds(source, 1), :], cap).astype(BF16)
+        hot = one_hot(rank_ref[pl.ds(planes[j], 1), :], cap).astype(BF16)
         stream = stream + dot_rows(hot, block)
     stream = stream.astype(BF16)
     stream_ref[...] = stream
@@ -368,8 +402,9 @@
     pall = whole.reshape(experts, GROUP, rows, whole.shape[1])
     for i in range(experts):
         pg[i] = pall[i].astype(BF16)
-    for i in range(experts):
-        go(p_copy(i))
+    outer = outer[::-1] + [0]
+    for j in outer:
+        go(p_copy(planes[j]))
 
     proj_in = jnp.dot(full[...], proj_ref[...], preferred_element_type=F32)
     norm_grad = proj_in * slope * gain
@@ -388,6 +423,19 @@
     def q_copy(j):
         return remote(pz_out.at[j], pz.at[j], q_send.at[j], q_recv.at[j], z_peers[j - 1])
 
+    def join(j):
+        target = planes[j]
+        p_copy(target).wait_recv()
+        piece = pg[target, g].astype(F32) + py[target].astype(F32)
+        if j:
+            pz_out[j] = piece.astype(BF16)
+            go(q_copy(j))
+        else:
+            pgrad_ref[...] = piece
+
+    ready = max(1, experts // 4)
+    for j in outer[:ready]:
+        join(j)
     for n, device in ((3, across), (4, far), (5, partner)):
         stat_copy(n, device, device[1]).wait_recv()
     total = stats[0]
@@ -408,16 +456,8 @@
     def _():
         halo_copy().start()
 
-    for i in range(experts):
-        p_copy(i).wait_recv()
-    for j in list(range(1, experts)) + [0]:
-        target = lax.rem(e + j, experts)
-        piece = pg[target, g].astype(F32) + py[target].astype(F32)
-        if j:
-            pz_out[j] = piece.astype(BF16)
-            go(q_copy(j))
-        else:
-            pgrad_ref[...] = piece
+    for j in outer[ready:]:
+        join(j)
 
     @pl.when(s < sp_ways - 1)
     def _():
@@ -435,7 +475,7 @@
     ggrad_ref[...] = (glu * value_ref[...].astype(F32) * in_sig * (1.0 - in_sig)).astype(BF16)
 
     total = pgrad_ref[...]
-    for j in range(1, experts):
+    for j in outer[:-1]:
         q_copy(j).wait_recv()
         total = total + pz[j].astype(F32)
     pgrad_ref[...] = total
@@ -476,8 +516,8 @@
         in_specs=[hbm] * len(arrays),
         out_specs=(vmem,) * 7,
         scratch_shapes=[
-            pltpu.VMEM((tok, quarter), BF16),
-            pltpu.VMEM((tok, quarter), BF16),
+            pltpu.VMEM((tok, width), BF16),
+            pltpu.VMEM((tok, width), BF16),
             *[pltpu.VMEM(a.shape, a.dtype) for a in (routes, weights, value, gate_in, normed, std, gain, taps, w_proj)],
             pltpu.VMEM((padded, tok), jnp.int32),
             pltpu.VMEM((padded, tok), F32),
@@ -509,10 +549,10 @@
             dma((4,)),
             dma((3,)),
             dma((7,)),
-            dma((experts,)),
-            dma((experts,)),
-            dma((experts, 9)),
-            dma((experts, 9)),
+            dma((experts, 2, 2, 2)),
+            dma((experts, 2, 2, 2)),
+            dma((experts, 2, 2)),
+            dma((experts, 2, 2)),
             dma((experts, PAIR)),
             dma((experts, PAIR)),
             dma((experts, 4)),

time: 88.1 us -> 82.9 us (0.941)
  Pallas kernels: 87.2 us -> 81.9 us
    pallas_call x1, Pallas kernels: 84.6 us -> 79.3 us  [mega(): pl.pallas_call(functools.partial(mega_kernel, experts, cap, taps.shape[0]...]
where the time goes in v2:
time: 82.9 us; the launch traced here: 82.7 us
  Pallas kernels  81.9 us (99%)
    pallas_call x1, Pallas kernels, mega(): pl.pallas_call(functools.partial(mega_kernel, experts, cap, taps.shape[0]...  79.3 us
    pallas_call x1, Pallas kernels, finish(): pl.pallas_call(functools.partial(finish_kernel, count), out_shape=tuple((...  2.58 us

profile of v2, /device:TPU:0, one launch (start us, length us, event | category | flops | bytes accessed | tf_op | source)
XLA Modules:
  0.0 82.7 jit_solution(6017133263628863491)
XLA Ops:
  0.6 79.3 %mega.1 = (bf16[448,2048]{1,0:T(8,128)(2,1)S(1)}, bf16[448,2048]{1,0:T(8,128)(2,1)S(1)}, bf16[448,2048]{1,0:T(8,128)(2,1)S(1)}, bf16[128,512]{1,0:T(8,128)(2,1)S...) custom-call(bf16[128,2048]{1,0:T(8,128)(2,1)} %h_hbm.1, ...), custom_call_target="tpu_custom_call" | custom-call | tf_op jit(solution)/shard_map/mega/pallas_call | solution.py:505
  80.0 2.6 %finish.1 = (bf16[448,2048]{1,0:T(8,128)(2,1)}, bf16[448,2048]{1,0:T(8,128)(2,1)}, bf16[448,2048]{1,0:T(8,128)(2,1)}, bf16[128,512]{1,0:T(8,128)(2,1)}, f32[256,...) custom-call(bf16[448,2048]{1,0:T(8,128)(2,1)S(1)} %get-tuple-element.21.refs_0_, ...), custom_call_target="tpu_custom_call" | custom-call | tf_op jit(solution)/shard_map/finish/pallas_call | solution.py:586

commit v3 on v2

--- a/solution.py
+++ b/solution.py
@@ -41,11 +41,13 @@
     return place
 
 
+def hail(devices):
+    for device in devices:
+        pl.semaphore_signal(pltpu.get_barrier_semaphore(), inc=1, device_id=device, device_id_type=MESH)
+
+
 def greet(devices):
-    barrier = pltpu.get_barrier_semaphore()
-    for device in devices:
-        pl.semaphore_signal(barrier, inc=1, device_id=device, device_id_type=MESH)
-    pl.semaphore_wait(barrier, len(devices))
+    pl.semaphore_wait(pltpu.get_barrier_semaphore(), len(devices))
 
 
 def remote(src, dst, send, recv, device):
@@ -99,6 +101,8 @@
     z_peers = [(planes[j] * GROUP + g, t) for j in range(1, experts)]
     before = (lax.rem(s + sp_ways - 1, sp_ways), t)
     after = (lax.rem(s + 1, sp_ways), t)
+    friends = z_peers + [across, beside, partner, far, before, after]
+    hail(friends)
     def fetch(sem, *pairs):
         return [pltpu.make_async_copy(src, dst, sem.at[n]) for n, (src, dst) in enumerate(pairs)]
 
@@ -172,14 +176,30 @@
     blocks = [list(range(c, min(c + step, experts))) for c in range(0, experts, step)]
     first_block, last_blocks = blocks[1], blocks[:1:-1]
     outer = [j for block in [first_block] + last_blocks + blocks[:1] for j in block if j]
-    for n, j in enumerate(outer):
+
+    def z_out(k, j):
+        return link(k, j, 0, 0, pack.at[j, k], spot(k, j, 0, 0), z_peers[j - 1])
+
+    def z_start(block):
+        for j in block:
+            for k in range(2):
+                z_out(k, j).start()
+
+    later = outer[len(first_block) :]
+    middle = (lax.rem(e, 4) + 1) // 2 == 1
+    for j in outer:
         hot, scale = chosen(j)
         pack[j, 0] = jnp.dot(hot, h_ref[:, cols_of(t)], preferred_element_type=F32).astype(BF16)
         pack[j, 1] = (jnp.dot(hot, cot_ref[:, cols_of(t)], preferred_element_type=F32) * scale).astype(BF16)
-        if not n:
-            greet(z_peers + [across, beside, partner, far, before, after])
-        for k in range(2):
-            go(link(k, j, 0, 0, pack.at[j, k], spot(k, j, 0, 0), z_peers[j - 1]))
+        sent.extend(z_out(k, j) for k in range(2))
+        if j == first_block[-1]:
+            greet(friends)
+            z_start(first_block)
+
+    @pl.when(middle)
+    def _():
+        z_start(later)
+
     hot, scale = chosen(0)
     here = loc(0, g, t)[0]
     buf[0, here, :] = jnp.dot(hot, h_ref[...], preferred_element_type=F32).astype(BF16)
@@ -233,6 +253,10 @@
         act[rows, :] = (silu_gate * pre_up).astype(BF16)
         gg[rows, :] = gate_grad
         ug[rows, :] = up_grad
+
+    def compute_back(j):
+        rows = rows_of(j)
+        gate_grad, up_grad = gg[rows, :], ug[rows, :]
         for lane in (1 - lo, lo):
             for h in range(PAIR):
                 cols = cols_of(h * PAIR + lane)
@@ -245,25 +269,38 @@
 
     width = full.shape[1]
     piece = 256
-    per_item = width // piece // 4
+    per_item = width // piece // 8
+    units = gw.shape[0]
 
     def weight_item(which, n):
-        if n == 0:
-            flipped[...] = (gg, ug, act)[which][...].T
-
-        @pl.loop(n * per_item, (n + 1) * per_item)
-        def _(i):
-            cols = pl.ds(pl.multiple_of(i * piece, piece), piece)
-            rows = buf[1 if which == 2 else 0, :, cols]
-            (gw, uw, dw)[which][:, cols] = jnp.dot(flipped[...], rows, preferred_element_type=F32).astype(BF16)
-
-    items = [(which, n) for which in range(3) for n in range(4)]
+        if which == 0:
+            if n == 0:
+                flipped[pl.ds(0, units), :] = gg[...].T
+                flipped[pl.ds(units, units), :] = ug[...].T
+
+            @pl.loop(n * per_item, (n + 1) * per_item)
+            def _(i):
+                cols = pl.ds(pl.multiple_of(i * piece, piece), piece)
+                both_grads = jnp.dot(flipped[...], buf[0, :, cols], preferred_element_type=F32).astype(BF16)
+                gw[:, cols] = both_grads[:units]
+                uw[:, cols] = both_grads[units:]
+        else:
+            if n == 0:
+                flipped[pl.ds(0, units), :] = act[...].T
+
+            @pl.loop(2 * n * per_item, 2 * (n + 1) * per_item)
+            def _(i):
+                cols = pl.ds(pl.multiple_of(i * piece, piece), piece)
+                dw[:, cols] = jnp.dot(
+                    flipped[pl.ds(0, units), :], buf[1, :, cols], preferred_element_type=F32
+                ).astype(BF16)
+
+    items = [(0, n) for n in range(8)] + [(1, n) for n in range(4)]
 
     def fill(count=1):
         for _ in range(count):
             if items:
-                which, n = items.pop(0)
-                weight_item(which, n)
+                weight_item(*items.pop(0))
 
     def core_copy(j, h, lane):
         return remote(
@@ -324,42 +361,50 @@
             for j in block:
                 stage(j)
 
-    def work(block):
-        if len(block) == 1:
-            compute(block[0])
-            return
-        pl.loop(block[0], block[-1] + 1)(compute)
-        for j in block:
-            for h in range(PAIR):
-                go(core_copy(j, h, 1 - lo))
+    def work(block, *stages):
+        for stage in stages:
+            if len(block) == 1:
+                stage(block[0])
+            else:
+                pl.loop(block[0], block[-1] + 1)(stage)
+        if len(block) > 1 and compute_back in stages:
+            for j in block:
+                for h in range(PAIR):
+                    go(core_copy(j, h, 1 - lo))
 
     own, near, far_one, far_two = blocks[0], first_block, *last_blocks
     d_first(0)
-    flow((d_first, near), (d_second, near), (d_first, own[1:]), (d_second, own), (d_third, near))
-    flow((d_last, near), (d_first, far_one))
+    flow((d_first, near))
+
+    @pl.when(jnp.logical_not(middle))
+    def _():
+        z_start(later)
+
+    flow((d_first, own[1:]), (d_second, own), (d_second, near), (d_first, far_one), (d_third, near))
+    flow((d_last, near), (d_first, far_two))
     for copy in loads:
         copy.wait()
-    work(near)
-    flow((d_third, own), (d_first, far_two), (d_last, own))
-    work(own)
-    flow((d_second, far_one), (d_second, far_two), (first, near), (first, own), (d_third, far_one), (d_last, far_one))
-    work(far_one)
-    flow((d_third, far_two), (first, far_one), (d_last, far_two), (second, near), (second, own))
-    work(far_two)
+    work(near, compute, compute_back)
+    flow((d_second, far_one), (d_third, own), (d_last, own))
+    work(own, compute)
+    flow((d_second, far_two), (first, near), (d_third, far_one), (d_last, far_one))
+    work(far_one, compute, compute_back)
+    flow((d_third, far_two), (first, far_one), (d_last, far_two), (second, near))
+    work(far_two, compute, compute_back)
     flow((first, far_two))
+    work(own, compute_back)
+    flow((second, far_one), (third, near))
+    fill(2)
+    flow((second, far_two), (first, own))
     fill(1)
-    flow((second, far_one))
-    fill(1)
-    flow((third, near))
-    fill(1)
-    flow((third, own))
-    fill(1)
-    flow((second, far_two))
-    fill(2)
     flow((third, far_one))
     fill(1)
     flow((third, far_two))
-    fill(len(items))
+    fill(1)
+    flow((second, own))
+    fill(2)
+    flow((third, own))
+    fill(1)
 
     for copy in extras:
         copy.wait()
@@ -371,7 +416,7 @@
     proj_act = (pre_act * act_sig).astype(BF16)
 
     stream = cot_ref[:, cols_of(t)].astype(F32)
-    for j in [0] + list(range(1, experts)):
+    for j in [0] + [k for block in (near, far_one, far_two, own[1:]) for k in block]:
         if j:
             z_copy(j).wait_recv()
             block = back[j]
@@ -386,27 +431,53 @@
     def gather_copy(n, col, device):
         return remote(full.at[:, cols_of(col)], full.at[:, cols_of(col)], t_send.at[n], t_recv.at[n], device)
 
+    rows = pg.shape[2]
+    share = experts // tp_ways
+
+    def p_copy(plane):
+        return remote(pg.at[plane, 1 - g], py.at[plane], p_send.at[plane], p_recv.at[plane], beside)
+
+    def q_copy(plane):
+        return remote(pz_out.at[plane], pz.at[e], q_send.at[plane], q_recv.at[e], (plane * GROUP + g, t))
+
+    def part(col):
+        block = full[:, cols_of(col)]
+        pall = dot_rows(block, proj_act).reshape(share, GROUP, rows, proj_act.shape[1]).astype(BF16)
+        for n in range(share):
+            pg[col * share + n] = pall[n]
+        for n in range(share):
+            go(p_copy(col * share + n))
+        taken = proj_ref[pl.ds(pl.multiple_of(col * quarter, quarter), quarter), :]
+        return jnp.dot(block, taken, preferred_element_type=F32)
+
+    def join(col):
+        for n in range(share):
+            plane = col * share + n
+            p_copy(plane).wait_recv()
+            piece = pg[plane, g].astype(F32) + py[plane].astype(F32)
+            pz_out[plane] = piece.astype(BF16)
+
+            @pl.when(plane == e)
+            def _():
+                pgrad_ref[...] = piece
+
+            @pl.when(plane != e)
+            def _():
+                q_copy(plane).start()
+
     go(gather_copy(0, t, across))
     go(gather_copy(1, t, partner))
-    gather_copy(0, across[1], across).wait_recv()
-    go(gather_copy(2, across[1], partner))
-    gather_copy(1, partner[1], partner).wait_recv()
-    gather_copy(2, far[1], partner).wait_recv()
-
-    rows = pg.shape[2]
-
-    def p_copy(j):
-        return remote(pg.at[j, 1 - g], py.at[j], p_send.at[j], p_recv.at[j], beside)
-
-    whole = dot_rows(full[...], proj_act)
-    pall = whole.reshape(experts, GROUP, rows, whole.shape[1])
-    for i in range(experts):
-        pg[i] = pall[i].astype(BF16)
-    outer = outer[::-1] + [0]
-    for j in outer:
-        go(p_copy(planes[j]))
-
-    proj_in = jnp.dot(full[...], proj_ref[...], preferred_element_type=F32)
+    proj_in = part(t)
+    gather_copy(1, other_t, partner).wait_recv()
+    proj_in = proj_in + part(other_t)
+    fill(1)
+    join(t)
+    gather_copy(0, across_t, across).wait_recv()
+    go(gather_copy(2, across_t, partner))
+    proj_in = proj_in + part(across_t)
+    join(other_t)
+    gather_copy(2, far_t, partner).wait_recv()
+    proj_in = proj_in + part(far_t)
     norm_grad = proj_in * slope * gain
     one = jnp.sum(norm_grad, axis=1, keepdims=True)
     two = jnp.sum(norm_grad * saved, axis=1, keepdims=True)
@@ -419,23 +490,8 @@
 
     for n, device in ((3, across), (4, far), (5, partner)):
         go(stat_copy(n, device, t))
-
-    def q_copy(j):
-        return remote(pz_out.at[j], pz.at[j], q_send.at[j], q_recv.at[j], z_peers[j - 1])
-
-    def join(j):
-        target = planes[j]
-        p_copy(target).wait_recv()
-        piece = pg[target, g].astype(F32) + py[target].astype(F32)
-        if j:
-            pz_out[j] = piece.astype(BF16)
-            go(q_copy(j))
-        else:
-            pgrad_ref[...] = piece
-
-    ready = max(1, experts // 4)
-    for j in outer[:ready]:
-        join(j)
+    fill(1)
+    join(across_t)
     for n, device in ((3, across), (4, far), (5, partner)):
         stat_copy(n, device, device[1]).wait_recv()
     total = stats[0]
@@ -456,8 +512,8 @@
     def _():
         halo_copy().start()
 
-    for j in outer[ready:]:
-        join(j)
+    join(far_t)
+    fill(len(items))
 
     @pl.when(s < sp_ways - 1)
     def _():
@@ -474,17 +530,21 @@
     vgrad_ref[...] = (glu * in_sig).astype(BF16)
     ggrad_ref[...] = (glu * value_ref[...].astype(F32) * in_sig * (1.0 - in_sig)).astype(BF16)
 
+    def q_arrival(j):
+        plane = planes[j]
+        return remote(pz_out.at[plane], pz.at[plane], q_send.at[plane], q_recv.at[plane], z_peers[j - 1])
+
     total = pgrad_ref[...]
-    for j in outer[:-1]:
-        q_copy(j).wait_recv()
-        total = total + pz[j].astype(F32)
+    for j in range(1, experts):
+        q_arrival(j).wait_recv()
+        total = total + pz[planes[j]].astype(F32)
     pgrad_ref[...] = total
 
     @pl.when(s > 0)
     def _():
         halo_copy().wait_send()
 
-    for copy in sent:
+    for copy in sent + [q_arrival(j) for j in range(1, experts)]:
         copy.wait_send()
 
 
@@ -529,7 +589,7 @@
             pltpu.VMEM((total, units), BF16),
             pltpu.VMEM((total, units), BF16),
             pltpu.VMEM((total, units), BF16),
-            pltpu.VMEM((units, total), BF16),
+            pltpu.VMEM((2 * units, total), BF16),
             pltpu.VMEM((total, width), BF16),
             pltpu.VMEM((experts, PAIR, GROUP * cap, quarter), BF16),
             pltpu.VMEM((2, experts, PAIR, GROUP, cap, half), BF16),

time: 82.9 us -> 75.6 us (0.912)
  Pallas kernels: 81.9 us -> 74.3 us
    pallas_call x1, Pallas kernels: 79.3 us -> 71.7 us  [mega(): pl.pallas_call(functools.partial(mega_kernel, experts, cap, taps.shape[0]...]
where the time goes in v3:
time: 75.6 us; the launch traced here: 75.1 us
  Pallas kernels  74.3 us (98%)
  between operations  0.81 us (1%)
    pallas_call x1, Pallas kernels, mega(): pl.pallas_call(functools.partial(mega_kernel, experts, cap, taps.shape[0]...  71.7 us
    pallas_call x1, Pallas kernels, finish(): pl.pallas_call(functools.partial(finish_kernel, count), out_shape=tuple((...  2.58 us

profile of v3, /device:TPU:0, one launch (start us, length us, event | category | flops | bytes accessed | tf_op | source)
XLA Modules:
  0.0 75.1 jit_solution(4131032169424090240)
XLA Ops:
  0.6 71.7 %mega.1 = (bf16[448,2048]{1,0:T(8,128)(2,1)S(1)}, bf16[448,2048]{1,0:T(8,128)(2,1)S(1)}, bf16[448,2048]{1,0:T(8,128)(2,1)S(1)}, bf16[128,512]{1,0:T(8,128)(2,1)S...) custom-call(bf16[128,2048]{1,0:T(8,128)(2,1)} %h_hbm.1, ...), custom_call_target="tpu_custom_call" | custom-call | tf_op jit(solution)/shard_map/mega/pallas_call | solution.py:565
  72.3 2.6 %finish.1 = (bf16[448,2048]{1,0:T(8,128)(2,1)}, bf16[448,2048]{1,0:T(8,128)(2,1)}, bf16[448,2048]{1,0:T(8,128)(2,1)}, bf16[128,512]{1,0:T(8,128)(2,1)}, f32[256,...) custom-call(bf16[448,2048]{1,0:T(8,128)(2,1)S(1)} %get-tuple-element.21.refs_0_, ...), custom_call_target="tpu_custom_call" | custom-call | tf_op jit(solution)/shard_map/finish/pallas_call | solution.py:646

commit v4 on v3

--- a/solution.py
+++ b/solution.py
@@ -185,7 +185,8 @@
             for k in range(2):
                 z_out(k, j).start()
 
-    later = outer[len(first_block) :]
+    far_one, far_two = last_blocks
+    rest = blocks[0][1:]
     middle = (lax.rem(e, 4) + 1) // 2 == 1
     for j in outer:
         hot, scale = chosen(j)
@@ -198,7 +199,7 @@
 
     @pl.when(middle)
     def _():
-        z_start(later)
+        z_start(far_one)
 
     hot, scale = chosen(0)
     here = loc(0, g, t)[0]
@@ -259,7 +260,7 @@
         gate_grad, up_grad = gg[rows, :], ug[rows, :]
         for lane in (1 - lo, lo):
             for h in range(PAIR):
-                cols = cols_of(h * PAIR + lane)
+                cols = cols_of(lane * PAIR + h)
                 grad_ref[rows, cols] = (
                     jnp.dot(gate_grad, wg[:, cols], preferred_element_type=F32)
                     + jnp.dot(up_grad, wu[:, cols], preferred_element_type=F32)
@@ -304,7 +305,7 @@
 
     def core_copy(j, h, lane):
         return remote(
-            grad_ref.at[rows_of(j), cols_of(h * PAIR + lane)],
+            grad_ref.at[rows_of(j), cols_of(lane * PAIR + h)],
             from_core.at[j, h], core_send.at[j, h], core_recv.at[j, h], partner,
         )
 
@@ -329,7 +330,7 @@
     def first(j):
         for h in range(PAIR):
             core_copy(j, h, lo).wait_recv()
-            mine = grad_ref[rows_of(j), cols_of(h * PAIR + lo)].astype(F32)
+            mine = grad_ref[rows_of(j), cols_of(lo * PAIR + h)].astype(F32)
             total = (mine + from_core[j, h].astype(F32)).astype(BF16).reshape(GROUP, cap, quarter)
             sums[0, j, h] = total[:, :, :half]
             sums[1, j, h] = total[:, :, half:]
@@ -372,39 +373,47 @@
                 for h in range(PAIR):
                     go(core_copy(j, h, 1 - lo))
 
-    own, near, far_one, far_two = blocks[0], first_block, *last_blocks
+    own, near = blocks[0], first_block
     d_first(0)
     flow((d_first, near))
 
+    @pl.when(middle)
+    def _():
+        z_start(far_two + rest)
+
+    flow((d_second, [0]))
+
     @pl.when(jnp.logical_not(middle))
     def _():
-        z_start(later)
-
-    flow((d_first, own[1:]), (d_second, own), (d_second, near), (d_first, far_one), (d_third, near))
+        z_start(far_one)
+
+    flow((d_second, near), (d_first, far_one))
+
+    @pl.when(jnp.logical_not(middle))
+    def _():
+        z_start(far_two + rest)
+
+    flow((d_third, near))
     flow((d_last, near), (d_first, far_two))
     for copy in loads:
         copy.wait()
     work(near, compute, compute_back)
-    flow((d_second, far_one), (d_third, own), (d_last, own))
+    flow((d_second, far_one), (d_first, rest), (d_second, rest), (d_third, own), (d_last, own))
     work(own, compute)
-    flow((d_second, far_two), (first, near), (d_third, far_one), (d_last, far_one))
+    flow((d_second, far_two), (first, near))
+    work(own, compute_back)
+    flow((d_third, far_one), (d_last, far_one), (first, own))
     work(far_one, compute, compute_back)
-    flow((d_third, far_two), (first, far_one), (d_last, far_two), (second, near))
+    flow((d_third, far_two), (first, far_one), (d_last, far_two), (second, near), (second, own))
     work(far_two, compute, compute_back)
-    flow((first, far_two))
-    work(own, compute_back)
-    flow((second, far_one), (third, near))
+    flow((second, far_one), (first, far_two), (third, near), (third, own))
     fill(2)
-    flow((second, far_two), (first, own))
-    fill(1)
     flow((third, far_one))
-    fill(1)
+    fill(2)
+    flow((second, far_two))
+    fill(2)
     flow((third, far_two))
-    fill(1)
-    flow((second, own))
-    fill(2)
-    flow((third, own))
-    fill(1)
+    fill(5)
 
     for copy in extras:
         copy.wait()
@@ -415,7 +424,9 @@
     slope = act_sig * (1.0 + pre_act * (1.0 - act_sig))
     proj_act = (pre_act * act_sig).astype(BF16)
 
-    stream = cot_ref[:, cols_of(t)].astype(F32)
+    own_q, other_q = lo * PAIR + hi, (1 - lo) * PAIR + hi
+    across_q, far_q = lo * PAIR + 1 - hi, (1 - lo) * PAIR + 1 - hi
+    stream = cot_ref[:, cols_of(own_q)].astype(F32)
     for j in [0] + [k for block in (near, far_one, far_two, own[1:]) for k in block]:
         if j:
             z_copy(j).wait_recv()
@@ -424,15 +435,18 @@
             block = done[0]
         hot = one_hot(rank_ref[pl.ds(planes[j], 1), :], cap).astype(BF16)
         stream = stream + dot_rows(hot, block)
-    stream = stream.astype(BF16)
-    stream_ref[...] = stream
-    full[:, cols_of(t)] = stream
-
-    def gather_copy(n, col, device):
-        return remote(full.at[:, cols_of(col)], full.at[:, cols_of(col)], t_send.at[n], t_recv.at[n], device)
+    full[:, cols_of(own_q)] = stream.astype(BF16)
+
+    def strip(col, n):
+        return pl.ds(pl.multiple_of(col * quarter + seq[n] * half, half), half)
+
+    def gather_copy(n, k, col, device):
+        ref = full.at[:, strip(col, n)]
+        return remote(ref, ref, t_send.at[2 * k + n], t_recv.at[2 * k + n], device)
 
     rows = pg.shape[2]
     share = experts // tp_ways
+    seq = (1 - g, g) if share == 1 else (0, 1)
 
     def p_copy(plane):
         return remote(pg.at[plane, 1 - g], py.at[plane], p_send.at[plane], p_recv.at[plane], beside)
@@ -440,15 +454,20 @@
     def q_copy(plane):
         return remote(pz_out.at[plane], pz.at[e], q_send.at[plane], q_recv.at[e], (plane * GROUP + g, t))
 
-    def part(col):
-        block = full[:, cols_of(col)]
-        pall = dot_rows(block, proj_act).reshape(share, GROUP, rows, proj_act.shape[1]).astype(BF16)
-        for n in range(share):
-            pg[col * share + n] = pall[n]
-        for n in range(share):
-            go(p_copy(col * share + n))
-        taken = proj_ref[pl.ds(pl.multiple_of(col * quarter, quarter), quarter), :]
-        return jnp.dot(block, taken, preferred_element_type=F32)
+    def part(col, n):
+        block = full[:, strip(col, n)]
+        pall = dot_rows(block, proj_act).astype(BF16)
+        if share == 1:
+            pg[col, seq[n]] = pall
+            planes_here = [col] * (1 - n)
+        else:
+            pall = pall.reshape(share // 2, GROUP, rows, proj_act.shape[1])
+            planes_here = [col * share + n * (share // 2) + m for m in range(share // 2)]
+            for m, plane in enumerate(planes_here):
+                pg[plane] = pall[m]
+        for plane in planes_here:
+            go(p_copy(plane))
+        return jnp.dot(block, proj_ref[strip(col, n), :], preferred_element_type=F32)
 
     def join(col):
         for n in range(share):
@@ -465,19 +484,21 @@
             def _():
                 q_copy(plane).start()
 
-    go(gather_copy(0, t, across))
-    go(gather_copy(1, t, partner))
-    proj_in = part(t)
-    gather_copy(1, other_t, partner).wait_recv()
-    proj_in = proj_in + part(other_t)
-    fill(1)
-    join(t)
-    gather_copy(0, across_t, across).wait_recv()
-    go(gather_copy(2, across_t, partner))
-    proj_in = proj_in + part(across_t)
-    join(other_t)
-    gather_copy(2, far_t, partner).wait_recv()
-    proj_in = proj_in + part(far_t)
+    for n in range(2):
+        go(gather_copy(n, 0, own_q, across))
+        go(gather_copy(n, 1, own_q, partner))
+    proj_in = part(own_q, 0) + part(own_q, 1)
+    for n in range(2):
+        gather_copy(n, 1, other_q, partner).wait_recv()
+        proj_in = proj_in + part(other_q, n)
+    for n in range(2):
+        gather_copy(n, 0, across_q, across).wait_recv()
+        go(gather_copy(n, 2, across_q, partner))
+        proj_in = proj_in + part(across_q, n)
+        join((own_q, other_q)[n])
+        gather_copy(n, 2, far_q, partner).wait_recv()
+        proj_in = proj_in + part(far_q, n)
+    stream_ref[...] = full[:, cols_of(t)]
     norm_grad = proj_in * slope * gain
     one = jnp.sum(norm_grad, axis=1, keepdims=True)
     two = jnp.sum(norm_grad * saved, axis=1, keepdims=True)
@@ -488,11 +509,11 @@
     def stat_copy(n, device, owner):
         return remote(stats.at[owner], stats.at[owner], t_send.at[n], t_recv.at[n], device)
 
-    for n, device in ((3, across), (4, far), (5, partner)):
+    for n, device in ((6, across), (7, far), (8, partner)):
         go(stat_copy(n, device, t))
-    fill(1)
-    join(across_t)
-    for n, device in ((3, across), (4, far), (5, partner)):
+    join(across_q)
+    join(far_q)
+    for n, device in ((6, across), (7, far), (8, partner)):
         stat_copy(n, device, device[1]).wait_recv()
     total = stats[0]
     for i in range(1, tp_ways):
@@ -506,13 +527,12 @@
     ext[pl.ds(0, tok), :] = conv
 
     def halo_copy():
-        return remote(ext.at[pl.ds(0, 32)], ext.at[pl.ds(tok, 32)], t_send.at[6], t_recv.at[6], before)
+        return remote(ext.at[pl.ds(0, 32)], ext.at[pl.ds(tok, 32)], t_send.at[9], t_recv.at[9], before)
 
     @pl.when(s > 0)
     def _():
         halo_copy().start()
 
-    join(far_t)
     fill(len(items))
 
     @pl.when(s < sp_ways - 1)
@@ -619,8 +639,8 @@
             dma((experts, 4)),
             dma((experts,)),
             dma((experts,)),
-            dma((7,)),
-            dma((7,)),
+            dma((10,)),
+            dma((10,)),
             dma((experts,)),
             dma((experts,)),
             dma((experts,)),

time: 75.6 us -> 74.4 us (0.984)
  Pallas kernels: 74.3 us -> 73.5 us
    pallas_call x1, Pallas kernels: 71.7 us -> 70.9 us  [mega(): pl.pallas_call(functools.partial(mega_kernel, experts, cap, taps.shape[0]...]
where the time goes in v4:
time: 74.4 us; the launch traced here: 74.3 us
  Pallas kernels  73.5 us (99%)
  between operations  0.81 us (1%)
    pallas_call x1, Pallas kernels, mega(): pl.pallas_call(functools.partial(mega_kernel, experts, cap, taps.shape[0]...  70.9 us
    pallas_call x1, Pallas kernels, finish(): pl.pallas_call(functools.partial(finish_kernel, count), out_shape=tuple((...  2.58 us

profile of v4, /device:TPU:0, one launch (start us, length us, event | category | flops | bytes accessed | tf_op | source)
XLA Modules:
  0.0 74.3 jit_solution(17769711764085782498)
XLA Ops:
  0.6 70.9 %mega.1 = (bf16[448,2048]{1,0:T(8,128)(2,1)S(1)}, bf16[448,2048]{1,0:T(8,128)(2,1)S(1)}, bf16[448,2048]{1,0:T(8,128)(2,1)S(1)}, bf16[128,512]{1,0:T(8,128)(2,1)S...) custom-call(bf16[128,2048]{1,0:T(8,128)(2,1)} %h_hbm.1, ...), custom_call_target="tpu_custom_call" | custom-call | tf_op jit(solution)/shard_map/mega/pallas_call | solution.py:585
  71.6 2.6 %finish.1 = (bf16[448,2048]{1,0:T(8,128)(2,1)}, bf16[448,2048]{1,0:T(8,128)(2,1)}, bf16[448,2048]{1,0:T(8,128)(2,1)}, bf16[128,512]{1,0:T(8,128)(2,1)}, f32[256,...) custom-call(bf16[448,2048]{1,0:T(8,128)(2,1)S(1)} %get-tuple-element.21.refs_0_, ...), custom_call_target="tpu_custom_call" | custom-call | tf_op jit(solution)/shard_map/finish/pallas_call | solution.py:666

commit v5 on v4

--- a/solution.py
+++ b/solution.py
@@ -199,7 +199,7 @@
 
     @pl.when(middle)
     def _():
-        z_start(far_one)
+        z_start(far_one + far_two + rest)
 
     hot, scale = chosen(0)
     here = loc(0, g, t)[0]
@@ -377,35 +377,27 @@
     d_first(0)
     flow((d_first, near))
 
-    @pl.when(middle)
-    def _():
-        z_start(far_two + rest)
-
     flow((d_second, [0]))
 
     @pl.when(jnp.logical_not(middle))
     def _():
-        z_start(far_one)
+        z_start(far_one + far_two + rest)
 
     flow((d_second, near), (d_first, far_one))
-
-    @pl.when(jnp.logical_not(middle))
-    def _():
-        z_start(far_two + rest)
-
-    flow((d_third, near))
+    flow((d_third, near), (d_third, [0]))
     flow((d_last, near), (d_first, far_two))
     for copy in loads:
         copy.wait()
     work(near, compute, compute_back)
-    flow((d_second, far_one), (d_first, rest), (d_second, rest), (d_third, own), (d_last, own))
-    work(own, compute)
+    flow((d_second, far_one), (d_first, rest), (d_second, rest), (d_third, rest), (d_last, own))
+    work(own, compute, compute_back)
     flow((d_second, far_two), (first, near))
-    work(own, compute_back)
     flow((d_third, far_one), (d_last, far_one), (first, own))
     work(far_one, compute, compute_back)
-    flow((d_third, far_two), (first, far_one), (d_last, far_two), (second, near), (second, own))
-    work(far_two, compute, compute_back)
+    flow((d_third, far_two), (first, far_one), (d_last, far_two), (second, near))
+    work(far_two, compute)
+    flow((second, own))
+    work(far_two, compute_back)
     flow((second, far_one), (first, far_two), (third, near), (third, own))
     fill(2)
     flow((third, far_one))
@@ -488,6 +480,7 @@
         go(gather_copy(n, 0, own_q, across))
         go(gather_copy(n, 1, own_q, partner))
     proj_in = part(own_q, 0) + part(own_q, 1)
+    fill(1)
     for n in range(2):
         gather_copy(n, 1, other_q, partner).wait_recv()
         proj_in = proj_in + part(other_q, n)

time: 74.4 us -> 72.9 us (0.980)
  Pallas kernels: 73.5 us -> 71.9 us
    pallas_call x1, Pallas kernels: 70.9 us -> 69.4 us  [mega(): pl.pallas_call(functools.partial(mega_kernel, experts, cap, taps.shape[0]...]
where the time goes in v5:
time: 72.9 us; the launch traced here: 72.7 us
  Pallas kernels  71.9 us (99%)
  between operations  0.81 us (1%)
    pallas_call x1, Pallas kernels, mega(): pl.pallas_call(functools.partial(mega_kernel, experts, cap, taps.shape[0]...  69.4 us
    pallas_call x1, Pallas kernels, finish(): pl.pallas_call(functools.partial(finish_kernel, count), out_shape=tuple((...  2.58 us

profile of v5, /device:TPU:0, one launch (start us, length us, event | category | flops | bytes accessed | tf_op | source)
XLA Modules:
  0.0 72.7 jit_solution(4325229382988613745)
XLA Ops:
  0.6 69.4 %mega.1 = (bf16[448,2048]{1,0:T(8,128)(2,1)S(1)}, bf16[448,2048]{1,0:T(8,128)(2,1)S(1)}, bf16[448,2048]{1,0:T(8,128)(2,1)S(1)}, bf16[128,512]{1,0:T(8,128)(2,1)S...) custom-call(bf16[128,2048]{1,0:T(8,128)(2,1)} %h_hbm.1, ...), custom_call_target="tpu_custom_call" | custom-call | tf_op jit(solution)/shard_map/mega/pallas_call | solution.py:578
  70.0 2.6 %finish.1 = (bf16[448,2048]{1,0:T(8,128)(2,1)}, bf16[448,2048]{1,0:T(8,128)(2,1)}, bf16[448,2048]{1,0:T(8,128)(2,1)}, bf16[128,512]{1,0:T(8,128)(2,1)}, f32[256,...) custom-call(bf16[448,2048]{1,0:T(8,128)(2,1)S(1)} %get-tuple-element.21.refs_0_, ...), custom_call_target="tpu_custom_call" | custom-call | tf_op jit(solution)/shard_map/finish/pallas_call | solution.py:659
